TPU v7x, 512 devices: a whole 4x8x8 slice. The times are simulated.
512 devices in a mesh: ep: 128 (over z, y, core), tp: 4 (over x).
Axes of the slice: x: 4, y: 8, z: 8, core: 2. Of those that a mesh axis runs over, the one named last changes fastest.
Arguments:
- tokens: bfloat16 [2048, 1024], P('ep'), may hold values from -24 to 24
- seq_length: int32 [2048], P('ep'), may hold values from 1024 to 16383
- ret_state: float32 [2048, 4, 128, 256], P('ep', 'tp'), may hold values from -0.6 to 0.6
- norm_in: float32 [1024], replicated, may hold values from 0.1 to 1.9
- w_query: bfloat16 [1024, 512], P(None, 'tp'), may hold values from -0.1875 to 0.1875
- w_key: bfloat16 [1024, 512], P(None, 'tp'), may hold values from -0.1875 to 0.1875
- w_value: bfloat16 [1024, 1024], P(None, 'tp'), may hold values from -0.1875 to 0.1875
- head_gain: float32 [1024], P('tp'), may hold values from 0.1 to 1.9
- w_output: bfloat16 [1024, 1024], P('tp'), may hold values from -0.1875 to 0.1875
- norm_mid: float32 [1024], replicated, may hold values from 0.1 to 1.9
- route_expert: int32 [2048, 2], P('ep'), may hold values from 0 to 63, all different within a row; in each aligned block of 16 rows (0 to 15, 16 to 31, ...) at most 2 rows name the same one
- route_score: float32 [2048, 2], P('ep'), may hold values from -6 to 6
- expert_gate: bfloat16 [128, 1024, 1792], P('ep', None, 'tp'), may hold values from -0.1875 to 0.1875
- expert_up: bfloat16 [128, 1024, 1792], P('ep', None, 'tp'), may hold values from -0.1875 to 0.1875
- expert_down: bfloat16 [128, 1792, 1024], P('ep', 'tp'), may hold values from -0.09375 to 0.09375
Outputs:
- mixed: bfloat16 [2048, 1024], P('ep', 'tp')
Inputs may be any that keep to these rules, and one draw needn't show every extreme that they name: `route_expert`: each row names 2 different experts; within the rows of one device no expert is named by more than 2 rows, and some device's rows name one expert exactly 2 times.
All inputs are finite; a program needn't handle non-finite values.
Results may differ from a plain program's by a relative error of at most 0.014.
Values may be sent and summed in bfloat16 or wider, within the bound.
A program may use at most 64 MiB of HBM per device.

v0:
```python
import jax
import jax.numpy as jnp
from jax import lax
from jax.sharding import PartitionSpec as P

DK = 128
DV = 256
SPREAD = 2
TOP_K = 2


EPS = 1e-06


def in_blocks(x, dim, devices):
    lengths = x.shape
    pieces = x.reshape(*lengths[:dim], devices, lengths[dim] // devices, *lengths[dim + 1 :])
    return jnp.moveaxis(pieces, dim, 0)


def summed_on_arrival(x, axis, dim):
    pieces = in_blocks(x, dim, lax.axis_size(axis))
    arrived = lax.all_to_all(pieces, axis, split_axis=0, concat_axis=0, tiled=True)
    return arrived.astype(jnp.float32).sum(axis=0)


def copy_for_each(x, axis):
    copies = jnp.broadcast_to(x, (lax.axis_size(axis), *x.shape))
    return lax.all_to_all(copies, axis, split_axis=0, concat_axis=0, tiled=True)


def over_copies(x, axis):
    return copy_for_each(x, axis).astype(jnp.float32).sum(axis=0)


def rotate(head_rows, positions):
    half_width = head_rows.shape[-1] // 2
    inverse = 10000.0 ** (-jnp.arange(half_width, dtype=jnp.float32) / half_width)
    angles = positions[:, None] * inverse[None, :]
    cosine = jnp.cos(angles)[:, None, :]
    sine_part = jnp.sin(angles)[:, None, :]
    first_half = head_rows[..., :half_width]
    second = head_rows[..., half_width:]
    return jnp.concatenate(
        [first_half * cosine - second * sine_part, first_half * sine_part + second * cosine],
        axis=-1,
    )


def body(
    tokens,
    seq_length,
    ret_state,
    norm_in,
    w_query,
    w_key,
    w_value,
    head_gain,
    w_output,
    norm_mid,
    route_expert,
    route_score,
    expert_gate,
    expert_up,
    expert_down,
):
    n_lanes = lax.axis_size("tp")
    n_groups = lax.axis_size("ep")
    lane_index = lax.axis_index("tp")
    local_rows = tokens.shape[0]
    width = tokens.shape[1]
    quarter = width // n_lanes
    heads_here = w_query.shape[1] // DK
    token_f = tokens.astype(jnp.float32)
    normed = (
        token_f * lax.rsqrt(jnp.mean(token_f * token_f, axis=-1, keepdims=True) + EPS) * norm_in
    ).astype(jnp.bfloat16)
    query_proj = jnp.dot(normed, w_query, preferred_element_type=jnp.float32).astype(jnp.bfloat16)
    key_proj = jnp.dot(normed, w_key, preferred_element_type=jnp.float32).astype(jnp.bfloat16)
    value_proj = jnp.dot(normed, w_value, preferred_element_type=jnp.float32).astype(jnp.bfloat16)
    positions = seq_length.astype(jnp.float32)
    q_rot = rotate(query_proj.astype(jnp.float32).reshape(local_rows, heads_here, DK), positions)
    k_rot = rotate(
        key_proj.astype(jnp.float32).reshape(local_rows, heads_here, DK), positions
    ) * DK ** (-0.5)
    value_rows = value_proj.astype(jnp.float32).reshape(local_rows, heads_here, DV)
    head_index = (lane_index * heads_here + jnp.arange(heads_here, dtype=jnp.int32)).astype(
        jnp.float32
    )
    decay_rate = 1.0 - jnp.exp2(-2.0 - 2.0 * head_index)
    carried = jnp.einsum("bhd,bhde->bhe", q_rot, ret_state)
    within = jnp.sum(q_rot * k_rot, axis=-1, keepdims=True) * value_rows
    retained = decay_rate[None, :, None] * carried + within
    centre = jnp.mean(retained, axis=-1, keepdims=True)
    variance = jnp.mean(jnp.square(retained - centre), axis=-1, keepdims=True)
    ret_out = ((retained - centre) * lax.rsqrt(variance + EPS)).reshape(local_rows, heads_here * DV)
    ret_out = (ret_out * head_gain).astype(jnp.bfloat16)
    partial_value = jnp.dot(ret_out, w_output, preferred_element_type=jnp.float32)
    experts_n = n_groups // SPREAD
    cap = min(local_rows, max(2, 3 * local_rows * TOP_K // (2 * experts_n)))
    flat_rows = route_expert.reshape(-1)
    onehot = (flat_rows[:, None] == jnp.arange(experts_n, dtype=jnp.int32)[None, :]).astype(
        jnp.int32
    )
    rank_index = jnp.sum((jnp.cumsum(onehot, axis=0) - onehot) * onehot, axis=1)
    slot_index = flat_rows * cap + rank_index
    chosen_slot = (
        slot_index[:, None] == jnp.arange(experts_n * cap, dtype=jnp.int32)[None, :]
    ).astype(jnp.float32)
    chosen_slot = chosen_slot.reshape(local_rows, TOP_K, experts_n * cap)
    placing = jnp.sum(chosen_slot, axis=1).astype(jnp.bfloat16)
    weights = jax.nn.softmax(route_score, axis=-1)
    combine = jnp.sum(chosen_slot * weights[:, :, None], axis=1)
    gate_rows = expert_gate[0]
    up_rows = expert_up[0]
    down_rows = expert_down[0]
    attended = over_copies(partial_value.astype(jnp.bfloat16), "tp").astype(jnp.float32)
    resid_full = (token_f + attended).astype(jnp.bfloat16)
    resid_f = resid_full.astype(jnp.float32)
    mid_full = (
        resid_f * lax.rsqrt(jnp.mean(resid_f * resid_f, axis=-1, keepdims=True) + EPS) * norm_mid
    ).astype(jnp.bfloat16)
    resid = lax.dynamic_slice_in_dim(resid_full, lane_index * quarter, quarter, 1)
    mid = lax.dynamic_slice_in_dim(mid_full, lane_index * quarter, quarter, 1)
    packed = jnp.einsum("re,rc->ec", placing, mid, preferred_element_type=jnp.float32).astype(
        jnp.bfloat16
    )
    packed = packed.reshape(experts_n, cap, quarter)
    send_buffer = jnp.repeat(packed, SPREAD, axis=0)
    received = lax.all_to_all(send_buffer, "ep", split_axis=0, concat_axis=0, tiled=True)
    groups, row_count, cols = received.shape
    piece_cols = lax.all_gather(received, "tp", axis=2, tiled=True)
    piece_width = piece_cols.shape[2]
    flat_in = piece_cols.reshape(groups * row_count, piece_width)
    gate_sum = jnp.dot(flat_in, gate_rows, preferred_element_type=jnp.float32)
    up_sum = jnp.dot(flat_in, up_rows, preferred_element_type=jnp.float32)
    hidden = (jax.nn.silu(gate_sum) * up_sum).astype(jnp.bfloat16)
    down_part = jnp.dot(hidden, down_rows, preferred_element_type=jnp.float32)
    share = summed_on_arrival(down_part.astype(jnp.bfloat16), "tp", 1)
    returned = share.astype(jnp.bfloat16).reshape(groups, row_count, share.shape[1])
    arrived = lax.all_to_all(returned, "ep", split_axis=0, concat_axis=0, tiled=True)
    part_total = jnp.sum(
        arrived.reshape(experts_n, SPREAD, cap, quarter).astype(jnp.float32), axis=1
    )
    expert_out = part_total.astype(jnp.bfloat16)
    expert_mix = jnp.dot(combine, expert_out.reshape(experts_n * cap, quarter).astype(jnp.float32))
    return (resid.astype(jnp.float32) + expert_mix).astype(jnp.bfloat16)


def solution(mesh):
    placed = (
        P("ep", None),
        P("ep"),
        P("ep", "tp", None, None),
        P(),
        P(None, "tp"),
        P(None, "tp"),
        P(None, "tp"),
        P("tp"),
        P("tp", None),
        P(),
        P("ep", None),
        P("ep", None),
        P("ep", None, "tp"),
        P("ep", None, "tp"),
        P("ep", "tp", None),
    )
    return jax.shard_map(body, mesh=mesh, in_specs=placed, out_specs=P("ep", "tp"), check_vma=False)
```

profile of v0, /device:TPU:1, one launch (start us, length us, event | category | flops | bytes accessed | tf_op | source)
XLA Modules:
  0.0 94.6 jit_solution(541615782359818185)
XLA Ops:
  0.1 0.8 convert_element_type.79
  0.9 1.0 %fusion.22 = f32[16]{0:T(128)S(1)} fusion(bf16[16,1024]{1,0:T(8,128)(2,1)} %param.15), kind=kLoop, calls=%fused_computation.35 | loop fusion | flops 49136 | bytes 32832 | tf_op jit(solution)/shard_map/reduce_sum | solution.py:76
  1.9 1.2 %fusion.10 = f32[16,1,128]{2,0,1:T(8,128)S(1)} fusion(bf16[1024,128]{1,0:T(8,128)(2,1)} %param.20, bf16[16,1024]{1,0:T(8,128)(2,1)} %param.15, f32[1024]{0:T(1024)} %param.18, f32[16]{0:T(128)S(1)} %add_rsqrt_fusion.2), kind=kOutput, calls=%fused_computation.18 | convolution fusion | flops 4263936 | bytes 307264 | tf_op jit(solution)/shard_map/dot_general | solution.py:79
  3.1 1.2 %fusion.8 = f32[16,1,128]{2,0,1:T(8,128)S(1)} fusion(bf16[1024,128]{1,0:T(8,128)(2,1)} %param.19, bf16[16,1024]{1,0:T(8,128)(2,1)} %param.15, f32[1024]{0:T(1024)} %param.18, f32[16]{0:T(128)S(1)} %add_rsqrt_fusion.2), kind=kOutput, calls=%fused_computation.16 | convolution fusion | flops 4263936 | bytes 307264 | tf_op jit(solution)/shard_map/dot_general | solution.py:78
  4.3 0.1 fusion.37
  4.5 0.2 fusion.45
  4.6 0.3 fusion.60
  4.9 0.3 fusion.59
  5.3 0.2 multiply_reduce_fusion.1
  5.5 0.2 convolution_convert_fusion.2
  5.7 0.7 broadcast_in_dim.4
  6.4 4.8 %all-to-all-start = ((bf16[4,16,1024]{2,1,0:T(8,128)(2,1)}), bf16[4,16,1024]{2,1,0:T(8,128)(2,1)S(1)}, u32[]{:S(2)}, u32[]{:S(2)}) async-start(bf16[4,16,1024]{2,1,0:T(8,128)(2,1)} %broadcast_in_dim.4), calls=%async_computation | async-start | bytes 262144 | tf_op jit(solution)/shard_map/all_to_all | solution.py:29
  11.2 0.1 copy.41
  11.3 0.1 eq.29
  11.6 0.2 select_reduce_fusion.1
  11.7 0.1 reduce_sum.122
  11.8 0.1 copy.42
  11.9 0.8 dynamic-slice
  12.7 0.1 convert_reduce_fusion.1
  12.8 3.2 %all-to-all-done = bf16[4,16,1024]{2,1,0:T(8,128)(2,1)S(1)} async-done(((bf16[4,16,1024]{2,1,0:T(8,128)(2,1)}), bf16[4,16,1024]{2,1,0:T(8,128)(2,1)S(1)}, u32[]{:S(2)}, u32[]{:S(2)}) %all-to-all-start) | async-done | bytes 131104 | tf_op jit(solution)/shard_map/all_to_all | solution.py:29
  16.0 0.1 multiply_reduce_fusion
  16.2 0.2 convolution_convert_fusion.1
  16.5 31.5 %all_to_all.20 = bf16[128,2,256]{2,1,0:T(2,128)(2,1)S(1)} all-to-all(bf16[128,2,256]{2,1,0:T(2,128)(2,1)S(1)} %bitcast.62), channel_id=1, replica_groups=mesh['ep'=128,'tp'=4] {'ep'}, dimensions={0} | all-to-all | bytes 262144 | tf_op jit(solution)/shard_map/all_to_all | solution.py:130
  48.0 9.7 %all_gather.3 = bf16[128,2,1024]{2,1,0:T(2,128)(2,1)S(1)} all-gather(bf16[128,2,256]{2,1,0:T(2,128)(2,1)S(1)} %all_to_all.20), channel_id=1, replica_groups=mesh['ep'=128,'tp'=4] {'tp'}, dimensions={2}, use_global_device_ids=true | all-gather | bytes 655360 | tf_op jit(solution)/shard_map/all_gather | solution.py:132
  57.8 0.2 reshape.276
  58.0 2.4 %fusion.14 = f32[256,448]{0,1:T(8,128)} fusion(bf16[256,1024]{1,0:T(8,128)(2,1)S(1)} %reshape.276, bf16[1,1024,448]{1,2,0:T(8,128)(2,1)} %param.27), kind=kOutput, calls=%fused_computation.21 | convolution fusion | flops 234881024 | bytes 1900544 | tf_op jit(solution)/shard_map/dot_general | solution.py:135
  60.4 2.9 %convolution_convert_fusion = bf16[256,1024]{1,0:T(8,128)(2,1)S(1)} fusion(bf16[256,1024]{1,0:T(8,128)(2,1)S(1)} %reshape.276, bf16[1,448,1024]{2,1,0:T(8,128)(2,1)} %param.29, bf16[1,1024,448]{1,2,0:T(8,128)(2,1)} %param.28, f32[256,448]{0,1:T(8,128)} %fusion.14), kind=kOutput, calls=%fused_computation.2 | convolution fusion | flops 470712320 | bytes 3342336 | tf_op jit(solution)/shard_map/dot_general | solution.py:138
  63.3 9.6 %all_to_all.21 = bf16[4,256,256]{2,1,0:T(8,128)(2,1)S(1)} all-to-all(bf16[4,256,256]{2,1,0:T(8,128)(2,1)S(1)} %bitcast.60), channel_id=1, replica_groups=mesh['ep'=128,'tp'=4] {'tp'}, dimensions={0} | all-to-all | bytes 1048576 | tf_op jit(solution)/shard_map/all_to_all | solution.py:23
  72.9 0.1 reduce_sum.127
  73.0 20.6 %all_to_all.22 = bf16[128,2,256]{2,1,0:T(2,128)(2,1)S(1)} all-to-all(bf16[128,2,256]{2,1,0:T(2,128)(2,1)S(1)} %reshape.278), channel_id=1, replica_groups=mesh['ep'=128,'tp'=4] {'ep'}, dimensions={0} | all-to-all | bytes 262144 | tf_op jit(solution)/shard_map/all_to_all | solution.py:141
  93.7 0.2 bitcast_reduce_fusion
  93.9 0.7 fusion.3
  (34 shorter events, 0.5 us)
Async XLA Ops:
  0.0 4.6 %copy-start = (f32[16,1,128,256]{3,2,1,0:T(8,128)S(1)}, f32[16,1,128,256]{3,2,1,0:T(8,128)}, u32[]{:S(2)}) copy-start(f32[16,1,128,256]{3,2,1,0:T(8,128)} %param.17) | copy-start | bytes 6291460
  0.0 4.9 %copy-start.2 = (bf16[16,1024]{1,0:T(8,128)(2,1)S(1)}, bf16[16,1024]{1,0:T(8,128)(2,1)}, u32[]{:S(2)}) copy-start(bf16[16,1024]{1,0:T(8,128)(2,1)} %param.15) | copy-start | bytes 98308
  0.0 4.9 %copy-start.7 = (f32[1024]{0:T(1024)S(1)}, f32[1024]{0:T(1024)}, u32[]{:S(2)}) copy-start(f32[1024]{0:T(1024)} %param.18) | copy-start | bytes 12292
  0.0 4.9 %copy-start.6 = (bf16[1024,256]{1,0:T(8,128)(2,1)S(1)}, bf16[1024,256]{1,0:T(8,128)(2,1)}, u32[]{:S(2)}) copy-start(bf16[1024,256]{1,0:T(8,128)(2,1)} %param.21) | copy-start | bytes 1572868
  0.0 5.4 %copy-start.1 = (bf16[256,1024]{1,0:T(8,128)(2,1)S(1)}, bf16[256,1024]{1,0:T(8,128)(2,1)}, u32[]{:S(2)}) copy-start(bf16[256,1024]{1,0:T(8,128)(2,1)} %param.23) | copy-start | bytes 1572868
  0.0 5.4 %copy-start.5 = (f32[256]{0:T(256)S(1)}, f32[256]{0:T(256)}, u32[]{:S(2)}) copy-start(f32[256]{0:T(256)} %param.22) | copy-start | bytes 3076
  3.1 8.1 %copy-start.3 = (f32[16,2]{0,1:T(2,128)S(1)}, f32[16,2]{0,1:T(2,128)}, u32[]{:S(2)}) copy-start(f32[16,2]{0,1:T(2,128)} %param.26) | copy-start | bytes 388
  3.1 8.2 %copy-start.4 = (s32[16,2]{0,1:T(2,128)S(1)}, s32[16,2]{0,1:T(2,128)}, u32[]{:S(2)}) copy-start(s32[16,2]{0,1:T(2,128)} %param.25) | copy-start | bytes 388
  6.4 9.7 %all-to-all-start = ((bf16[4,16,1024]{2,1,0:T(8,128)(2,1)}), bf16[4,16,1024]{2,1,0:T(8,128)(2,1)S(1)}, u32[]{:S(2)}, u32[]{:S(2)}) async-start(bf16[4,16,1024]{2,1,0:T(8,128)(2,1)} %broadcast_in_dim.4), calls=%async_computation | async-start | bytes 262144 | tf_op jit(solution)/shard_map/all_to_all | solution.py:29
where the time goes:
time: 95 us; the launch traced here: 94.6 us
  blocking collectives  71.5 us (75%)
  matrix products  9.44 us (10%)
  starting transfers between devices  4.83 us (5%)
  waiting for transfers between devices  3.24 us (3%)
  other arithmetic  3.14 us (3%)
  local copies, waits for them, and re-layouts  2.24 us (2%)
    all_to_all x1, blocking collectives, body(): lax.all_to_all(send_buffer, 'ep', split_axis=0, concat_axis=0, tiled=True)  31.5 us
    all_to_all x1, blocking collectives, body(): lax.all_to_all(returned, 'ep', split_axis=0, concat_axis=0, tiled=True)  20.6 us
    all_gather x1, blocking collectives, body(): piece_cols = lax.all_gather(received, 'tp', axis=2, tiled=True)  9.74 us
    all_to_all x1, blocking collectives, summed_on_arrival(): lax.all_to_all(pieces, axis, split_axis=0, concat_axis=0, tiled=True)  9.56 us
    all_to_all x1, starting transfers between devices, copy_for_each(): return lax.all_to_all(copies, axis, split_axis=0, concat_axis=0, tiled=True)  4.83 us
    all_to_all x1, waiting for transfers between devices, copy_for_each(): return lax.all_to_all(copies, axis, split_axis=0, concat_axis=0, tiled=True)  3.24 us
    dot_general x1, matrix products, body(): down_part = jnp.dot(hidden, down_rows, preferred_element_type=jnp.float32)  2.9 us
    dot_general x1, matrix products, body(): gate_sum = jnp.dot(flat_in, gate_rows, preferred_element_type=jnp.float32)  2.4 us
  transfers between devices with their start and end apart: 1, of which 1 were waited for; matrix products, arithmetic and copies ran while one was open for 2% of the time, Pallas kernels for 0%

commit v1 on v0

v1 whole, which is shorter than its diff:
```python
import functools

import jax
import jax.numpy as jnp
from jax import lax
from jax.experimental import pallas as pl
from jax.experimental.pallas import tpu as pltpu
from jax.sharding import PartitionSpec as P

EPS = 1e-06
MESH = pl.DeviceIdType.MESH
F32 = jnp.float32
BF16 = jnp.bfloat16


def dot(a, b):
    return jnp.dot(a, b, preferred_element_type=F32)


def dot_rows(a, b):
    return lax.dot_general(a, b, (((0,), (0,)), ((), ())), preferred_element_type=F32)


def split(x):
    high = x.astype(BF16)
    return high, (x - high.astype(F32)).astype(BF16)


def to_blocks(x):
    rows = x.shape[0]
    return [x[:, 128 * h : 128 * (h + 1)].reshape(rows // 2, 2, 128) for h in range(2)]


def from_blocks(ref):
    blocks = ref.shape[1]
    return jnp.concatenate([ref[h].reshape(2 * blocks, 128) for h in range(2)], axis=1)


def kernel(
    n_ep,
    n_tp,
    tokens_h, seq_h, norm_in_h, wq_h, wk_h, wv_h, state_h, gain_h, wo_h, norm_mid_h,
    route_h, score_h, gate_h, up_h, down_h,
    out_ref,
    tokens, seq, norm_in, wq, wk, wv, state, gain, wo, norm_mid, route, score, gate, up, down,
    carried, a_send, a_recv, b_send, rows, hidden, own, d_send, d_recv, x_send, x_recv, e_send, e_recv,
    load_sem, a_ssem, a_rsem, b_ssem, b_rsem, g_ssem, g_rsem, f_ssem, f_rsem, d_ssem, d_rsem,
    x_ssem, x_rsem, e_ssem, e_rsem,
):
    chips = n_ep // 2
    ep = lax.axis_index("ep")
    tp = lax.axis_index("tp")
    chip = ep // 2
    core = lax.rem(ep, 2)
    other = 1 - core

    def peer(d):
        return lax.rem(tp + d, n_tp)

    def far(r):
        return lax.rem(chip + r, chips)

    sources = (tokens_h, seq_h, norm_in_h, wq_h, wk_h, wv_h, state_h, gain_h, wo_h, norm_mid_h,
               route_h, score_h, gate_h, up_h, down_h)
    places = (tokens, seq, norm_in, wq, wk, wv, state, gain, wo, norm_mid, route, score, gate, up, down)
    loads = [pltpu.make_async_copy(s, p, load_sem.at[i]) for i, (s, p) in enumerate(zip(sources, places))]
    (l_tokens, l_seq, l_norm_in, l_wq, l_wk, l_wv, l_state, l_gain, l_wo, l_norm_mid, l_route, l_score,
     l_gate, l_up, l_down) = loads
    for load in (l_tokens, l_norm_in, l_seq, l_wq, l_wk, l_wv, l_route, l_score, l_state, l_gain, l_wo,
                 l_norm_mid, l_gate, l_up, l_down):
        load.start()

    barrier = pltpu.get_barrier_semaphore()

    def greet(r, carry):
        pl.semaphore_signal(barrier, inc=1, device_id={"ep": far(r) * 2 + core, "tp": tp}, device_id_type=MESH)
        return carry

    lax.fori_loop(1, chips, greet, 0)
    for d in range(1, n_tp):
        pl.semaphore_signal(barrier, inc=1, device_id={"ep": ep, "tp": peer(d)}, device_id_type=MESH)
    pl.semaphore_signal(barrier, inc=1, device_id={"ep": chip * 2 + other, "tp": tp}, device_id_type=MESH)

    l_tokens.wait()
    l_norm_in.wait()
    token_f = tokens[...].astype(F32)
    normed = (
        token_f * lax.rsqrt(jnp.mean(token_f * token_f, axis=-1, keepdims=True) + EPS) * norm_in[...]
    ).astype(BF16)
    l_seq.wait()
    l_route.wait()
    l_score.wait()
    n_rows = token_f.shape[0]
    sub = lax.broadcasted_iota(jnp.int32, (n_rows, n_rows), 0)
    lane = lax.broadcasted_iota(jnp.int32, (n_rows, n_rows), 1)
    positions = jnp.sum(jnp.where(sub == lane, seq[...].astype(F32), 0.0), axis=1, keepdims=True)
    key_lane = lax.broadcasted_iota(jnp.int32, (n_rows, 128), 1)
    pair = lax.rem(key_lane, 64).astype(F32)
    angles = positions * jnp.exp(pair * (-jnp.log(10000.0) / 64.0))
    cosine = jnp.cos(angles)
    sine = jnp.where(key_lane < 64, -1.0, 1.0) * jnp.sin(angles)

    experts = chips
    expert_lane = lax.broadcasted_iota(jnp.int32, (n_rows, 2 * experts), 1)
    choice = [route[:, k : k + 1] for k in range(2)]
    named = [(expert_lane == c).astype(F32) for c in choice]
    earlier = dot((lane < sub).astype(BF16), (named[0] + named[1]).astype(BF16))
    picked = []
    for k in range(2):
        rank = jnp.sum(earlier * named[k], axis=1, keepdims=True).astype(jnp.int32)
        picked.append((expert_lane == choice[k] * 2 + rank).astype(F32))
    placing = (picked[0] + picked[1]).astype(BF16)
    top = jnp.max(score[...], axis=1, keepdims=True)
    grown = jnp.exp(score[...] - top)
    weights = grown / jnp.sum(grown, axis=1, keepdims=True)
    combine = picked[0] * weights[:, 0:1] + picked[1] * weights[:, 1:2]
    combine_high, combine_low = split(combine)

    def rotate(x):
        return x * cosine + pltpu.roll(x, 64, 1) * sine

    l_wq.wait()
    q_rot = rotate(dot(normed, wq[...]).astype(BF16).astype(F32))
    l_wk.wait()
    k_rot = rotate(dot(normed, wk[...]).astype(BF16).astype(F32)) * (128.0 ** -0.5)
    l_wv.wait()
    value_rows = dot(normed, wv[...]).astype(BF16).astype(F32)
    within = jnp.sum(q_rot * k_rot, axis=-1, keepdims=True) * value_rows
    q_cols = q_rot.T
    l_state.wait()
    for b in range(n_rows):
        carried[b : b + 1, :] = jnp.sum(q_cols[:, b : b + 1] * state[b, 0], axis=0, keepdims=True)
    head = jnp.full((1, 1), tp, jnp.int32).astype(F32)
    decay = 1.0 - jnp.exp2(-2.0 - 2.0 * head)
    retained = decay * carried[...] + within
    centred = retained - jnp.mean(retained, axis=-1, keepdims=True)
    variance = jnp.mean(centred * centred, axis=-1, keepdims=True)
    l_gain.wait()
    ret_out = (centred * lax.rsqrt(variance + EPS) * gain[...]).astype(BF16)
    l_wo.wait()
    width = out_ref.shape[1]
    mine = pl.ds(pl.multiple_of(tp * width, 128), width)

    order = [2, 1, 3]
    for d in order:
        columns = pl.ds(pl.multiple_of(peer(d) * width, 128), width)
        a_send[d] = dot(ret_out, wo[:, columns]).astype(BF16)
    own_part = dot(ret_out, wo[:, mine]).astype(BF16).astype(F32)

    pl.semaphore_wait(barrier, chips - 1 + n_tp - 1 + 1)
    a_copies = {}
    for d in order:
        a_copies[d] = pltpu.make_async_remote_copy(
            src_ref=a_send.at[d], dst_ref=a_recv.at[d], send_sem=a_ssem.at[d], recv_sem=a_rsem.at[d],
            device_id={"ep": ep, "tp": peer(d)}, device_id_type=MESH,
        )
        a_copies[d].start()
    attended = own_part
    for d in (1, 3, 2):
        a_copies[d].wait_recv()
        attended = attended + a_recv[d].astype(F32)
    resid = (tokens[:, mine].astype(F32) + attended).astype(BF16)

    packed = dot_rows(placing, resid).astype(BF16)
    for h, part in enumerate(to_blocks(packed)):
        b_send[h] = part

    here = rows.at[tp, core]

    def send_rows(r, carry):
        target = far(r)
        pltpu.make_async_remote_copy(
            src_ref=b_send.at[:, target], dst_ref=here.at[:, r], send_sem=b_ssem, recv_sem=b_rsem,
            device_id={"ep": target * 2 + core, "tp": tp}, device_id_type=MESH,
        ).start()
        return carry

    lax.fori_loop(1, chips, send_rows, 0)
    for h in range(2):
        rows[tp, core, h, 0] = b_send[h, chip]
    rest = pl.ds(1, chips - 1)
    all_rows = pltpu.make_async_remote_copy(
        src_ref=b_send.at[:, rest], dst_ref=here.at[:, rest], send_sem=b_ssem, recv_sem=b_rsem,
        device_id={"ep": ep, "tp": peer(1)}, device_id_type=MESH,
    )
    all_rows.wait_recv()

    g_copies = {}
    for d in order:
        g_copies[d] = pltpu.make_async_remote_copy(
            src_ref=here, dst_ref=here, send_sem=g_ssem.at[d], recv_sem=g_rsem.at[d],
            device_id={"ep": ep, "tp": peer(d)}, device_id_type=MESH,
        )
        g_copies[d].start()

    f_copies = {}

    def forward(d):
        block = rows.at[peer(n_tp - d), core] if d else here
        f_copies[d] = pltpu.make_async_remote_copy(
            src_ref=block, dst_ref=block, send_sem=f_ssem.at[d], recv_sem=f_rsem.at[d],
            device_id={"ep": chip * 2 + other, "tp": tp}, device_id_type=MESH,
        )
        f_copies[d].start()

    forward(0)
    l_norm_mid.wait()
    l_gate.wait()
    l_up.wait()
    squares = [None, None]
    gates = [None, None]
    ups = [None, None]

    def take(side, d):
        source = peer(n_tp - d) if d else tp
        x = from_blocks(rows.at[source, core if side == 0 else other]).astype(F32)
        columns = pl.ds(pl.multiple_of(source * width, 128), width)
        part = jnp.sum(x * x, axis=-1, keepdims=True)
        y = (x * norm_mid[:, columns]).astype(BF16)
        g = dot(y, gate[0, columns, :])
        u = dot(y, up[0, columns, :])
        squares[side] = part if squares[side] is None else squares[side] + part
        gates[side] = g if gates[side] is None else gates[side] + g
        ups[side] = u if ups[side] is None else ups[side] + u

    take(0, 0)
    for d in (1, 3, 2):
        g_copies[d].wait_recv()
        forward(d)
        take(0, d)
    for d in (0, 1, 3, 2):
        f_copies[d].wait_recv()
        take(1, d)
    half = 2 * chips
    for side in range(2):
        scale = lax.rsqrt(squares[side] * (1.0 / (n_tp * width)) + EPS)
        g = gates[side] * scale
        u = ups[side] * scale
        hidden[side] = (g / (1.0 + jnp.exp(-g)) * u).astype(BF16)

    l_down.wait()
    d_copies = {}
    for d in (2, 1, 3, 0):
        columns = pl.ds(pl.multiple_of(peer(d) * width, 128), width)
        d_send[d] = dot(hidden[1], down[0, :, columns]).astype(BF16)
        d_copies[d] = pltpu.make_async_remote_copy(
            src_ref=d_send.at[d], dst_ref=d_recv.at[d], send_sem=d_ssem.at[d], recv_sem=d_rsem.at[d],
            device_id={"ep": chip * 2 + other, "tp": tp}, device_id_type=MESH,
        )
        d_copies[d].start()
        own[d] = dot(hidden[0], down[0, :, columns])
    x_copies = {}
    for d in order:
        d_copies[d].wait_recv()
        x_send[d] = (own[d] + d_recv[d].astype(F32)).astype(BF16)
        x_copies[d] = pltpu.make_async_remote_copy(
            src_ref=x_send.at[d], dst_ref=x_recv.at[d], send_sem=x_ssem.at[d], recv_sem=x_rsem.at[d],
            device_id={"ep": ep, "tp": peer(d)}, device_id_type=MESH,
        )
        x_copies[d].start()
    d_copies[0].wait_recv()
    total = own[0] + d_recv[0].astype(F32)
    for d in (1, 3, 2):
        x_copies[d].wait_recv()
        total = total + x_recv[d].astype(F32)
    for h, part in enumerate(to_blocks(total.astype(BF16))):
        e_send[h] = part

    def send_back(r, carry):
        target = far(chips - r)
        pltpu.make_async_remote_copy(
            src_ref=e_send.at[:, r], dst_ref=e_recv.at[:, chip], send_sem=e_ssem, recv_sem=e_rsem,
            device_id={"ep": target * 2 + core, "tp": tp}, device_id_type=MESH,
        ).start()
        return carry

    lax.fori_loop(1, chips, send_back, 0)
    for h in range(2):
        e_recv[h, chip] = e_send[h, 0]
    all_back = pltpu.make_async_remote_copy(
        src_ref=e_send.at[:, rest], dst_ref=e_recv.at[:, rest], send_sem=e_ssem, recv_sem=e_rsem,
        device_id={"ep": ep, "tp": peer(1)}, device_id_type=MESH,
    )
    all_back.wait_recv()
    back = from_blocks(e_recv)
    mix = dot(combine_high, back) + dot(combine_low, back)
    out_ref[...] = (resid.astype(F32) + mix).astype(BF16)

    all_rows.wait_send()
    all_back.wait_send()
    for d in order:
        a_copies[d].wait_send()
        g_copies[d].wait_send()
        x_copies[d].wait_send()
    for d in range(n_tp):
        f_copies[d].wait_send()
        d_copies[d].wait_send()


def body(
    n_ep, n_tp, tokens, seq_length, ret_state, norm_in, w_query, w_key, w_value, head_gain, w_output,
    norm_mid, route_expert, route_score, expert_gate, expert_up, expert_down,
):
    n_rows, model = tokens.shape
    chips = n_ep // 2
    width = model // n_tp
    args = (
        tokens, seq_length.reshape(1, -1), norm_in.reshape(1, -1), w_query, w_key, w_value, ret_state,
        head_gain.reshape(1, -1), w_output, norm_mid.reshape(1, -1), route_expert, route_score,
        expert_gate, expert_up, expert_down,
    )
    dma = pltpu.SemaphoreType.DMA
    blocks = (2, chips, 2, width // 2)
    scratch = [pltpu.VMEM(a.shape, a.dtype) for a in args] + [
        pltpu.VMEM((n_rows, head_gain.shape[0]), F32),
        pltpu.VMEM((n_tp, n_rows, width), BF16),
        pltpu.VMEM((n_tp, n_rows, width), BF16),
        pltpu.VMEM(blocks, BF16),
        pltpu.VMEM((n_tp, 2) + blocks, BF16),
        pltpu.VMEM((2, 2 * chips, expert_down.shape[1]), BF16),
        pltpu.VMEM((n_tp, 2 * chips, width), F32),
        pltpu.VMEM((n_tp, 2 * chips, width), BF16),
        pltpu.VMEM((n_tp, 2 * chips, width), BF16),
        pltpu.VMEM((n_tp, 2 * chips, width), BF16),
        pltpu.VMEM((n_tp, 2 * chips, width), BF16),
        pltpu.VMEM(blocks, BF16),
        pltpu.VMEM(blocks, BF16),
        dma((len(args),)),
        dma((n_tp,)), dma((n_tp,)),
        dma, dma,
        dma((n_tp,)), dma((n_tp,)),
        dma((n_tp,)), dma((n_tp,)),
        dma((n_tp,)), dma((n_tp,)),
        dma((n_tp,)), dma((n_tp,)),
        dma, dma,
    ]
    return pl.pallas_call(
        functools.partial(kernel, n_ep, n_tp),
        out_shape=jax.ShapeDtypeStruct((n_rows, width), BF16),
        in_specs=[pl.BlockSpec(memory_space=pl.ANY)] * len(args),
        out_specs=pl.BlockSpec(memory_space=pltpu.VMEM),
        scratch_shapes=scratch,
        compiler_params=pltpu.CompilerParams(collective_id=0, has_side_effects=True),
        name="step",
    )(*args)


def solution(mesh):
    placed = (
        P("ep", None),
        P("ep"),
        P("ep", "tp", None, None),
        P(),
        P(None, "tp"),
        P(None, "tp"),
        P(None, "tp"),
        P("tp"),
        P("tp", None),
        P(),
        P("ep", None),
        P("ep", None),
        P("ep", None, "tp"),
        P("ep", None, "tp"),
        P("ep", "tp", None),
    )
    step = functools.partial(body, mesh.shape["ep"], mesh.shape["tp"])
    return jax.shard_map(step, mesh=mesh, in_specs=placed, out_specs=P("ep", "tp"), check_vma=False)
```

time: 95 us -> 57.5 us (0.61)
  blocking collectives: 71.5 us -> 0 us
  Pallas kernels: 0 us -> 49.6 us
  matrix products: 9.44 us -> 0 us
  local copies, waits for them, and re-layouts: 2.24 us -> 7.65 us
  starting transfers between devices: 4.83 us -> 0 us
  waiting for transfers between devices: 3.24 us -> 0 us
  other arithmetic: 3.14 us -> 0 us
    all_to_all x3 -> x0, blocking collectives: 61.7 us -> none  [the longest x1 31.5 us: body(): lax.all_to_all(send_buffer, 'ep', split_axis=0, concat_axis=0, tiled=True)]
    pallas_call x0 -> x1, Pallas kernels: none -> 49.6 us  [body(): pl.pallas_call(functools.partial(kernel, n_ep, n_tp), out_shape=jax.Shape...]
    all_gather x1 -> x0, blocking collectives: 9.74 us -> none  [body(): piece_cols = lax.all_gather(received, 'tp', axis=2, tiled=True)]
    dot_general x9 -> x0, matrix products: 9.44 us -> none  [the longest x1 2.9 us: body(): down_part = jnp.dot(hidden, down_rows, preferred_element_type=jnp.float32)]
    unnamed x17 -> x7, local copies, waits for them, and re-layouts: 0.12 us -> 7.65 us
    all_to_all x1 -> x0, starting transfers between devices: 4.83 us -> none  [copy_for_each(): return lax.all_to_all(copies, axis, split_axis=0, concat_axis=0, tiled=True)]
    all_to_all x1 -> x0, waiting for transfers between devices: 3.24 us -> none  [copy_for_each(): return lax.all_to_all(copies, axis, split_axis=0, concat_axis=0, tiled=True)]
    reduce_sum x10 -> x0, other arithmetic: 1.99 us -> none  [the longest x1 0.96 us: body(): jnp.mean(token_f * token_f, axis=-1, keepdims=True) + EPS]
  transfers between devices with their start and end apart: 1 -> 0, of which waited for: 1 -> 0; matrix products, arithmetic and copies ran while one was open for 2% -> 0% of each run, Pallas kernels for 0% -> 0%
where the time goes in v1:
time: 57.5 us; the launch traced here: 57.3 us
  Pallas kernels  49.6 us (86%)
  local copies, waits for them, and re-layouts  7.65 us (13%)
    pallas_call x1, Pallas kernels, body(): pl.pallas_call(functools.partial(kernel, n_ep, n_tp), out_shape=jax.Shape...  49.6 us
    unnamed x7, local copies, waits for them, and re-layouts  7.65 us

profile of v1, /device:TPU:1, one launch (start us, length us, event | category | flops | bytes accessed | tf_op | source)
XLA Modules:
  0.0 57.3 jit_solution(5344993410568828358)
XLA Ops:
  0.0 0.0 copy-start
  0.0 1.4 %copy.16.route_h = s32[16,2]{1,0:T(8,128)} copy(s32[16,2]{0,1:T(2,128)} %param.25) | data formatting | bytes 256 | tf_op args[10]
  1.4 1.3 %copy.17.score_h = f32[16,2]{1,0:T(8,128)} copy(f32[16,2]{0,1:T(2,128)} %param.26) | data formatting | bytes 256 | tf_op args[11]
  2.8 2.3 %copy.18.gate_h = bf16[1,1024,448]{2,1,0:T(8,128)(2,1)} copy(bf16[1,1024,448]{1,2,0:T(8,128)(2,1)} %param.27) | data formatting | bytes 1835008 | tf_op args[12]
  5.0 0.0 copy-done
  5.0 1.3 %copy.19.up_h = bf16[1,1024,448]{2,1,0:T(8,128)(2,1)} copy(bf16[1,1024,448]{1,2,0:T(8,128)(2,1)S(1)} %copy-done) | data formatting | bytes 1835008 | tf_op args[13]
  6.4 49.6 %step.1 = bf16[16,256]{1,0:T(8,128)(2,1)} custom-call(bf16[16,1024]{1,0:T(8,128)(2,1)} %tokens_h.1, s32[1,16]{1,0:T(1,128)} %bitcast.7, f32[1,1024]{1,0:T(1,128)} %bitcast.4, bf16[1024,128]{1,0:T(8,128)(2,1)} %wq_h.1, bf16[1024,128]{1,0:T(8,128)(2,1)} %wk_h.1, bf16[1024,256]{1,0:T(8,128)(2,1)} %wv_h.1, f32[16,1,128,256]{3,2,1,0:T(8,128)} %state_h.1, ...), custom_call_target="tpu_custom_call" | custom-call | tf_op jit(solution)/shard_map/step/pallas_call | solution.py:337
  56.0 1.3 %copy.21 = bf16[16,256]{1,0:T(8,128)(2,1)} copy(bf16[16,256]{1,0:T(8,128)(2,1)} %step.1) | data formatting | bytes 16384
Async XLA Ops:
  0.0 5.0 %copy-start = (bf16[1,1024,448]{1,2,0:T(8,128)(2,1)S(1)}, bf16[1,1024,448]{1,2,0:T(8,128)(2,1)}, u32[]{:S(2)}) copy-start(bf16[1,1024,448]{1,2,0:T(8,128)(2,1)} %param.28) | copy-start | bytes 2752516

commit v2 on v1

v2 whole, which is shorter than its diff:
```python
import functools

import jax
import jax.numpy as jnp
from jax import lax
from jax.experimental import pallas as pl
from jax.experimental.pallas import tpu as pltpu
from jax.sharding import PartitionSpec as P

EPS = 1e-06
MESH = pl.DeviceIdType.MESH
F32 = jnp.float32
BF16 = jnp.bfloat16


def dot(a, b):
    return jnp.dot(a, b, preferred_element_type=F32)


def dot_cols(a, b):
    return lax.dot_general(a, b, (((1,), (1,)), ((), ())), preferred_element_type=F32)


def dot_rows(a, b):
    return lax.dot_general(a, b, (((0,), (0,)), ((), ())), preferred_element_type=F32)


def split(x):
    high = x.astype(BF16)
    return high, (x - high.astype(F32)).astype(BF16)


def to_blocks(x):
    rows = x.shape[0]
    return [x[:, 128 * h : 128 * (h + 1)].reshape(rows // 2, 2, 128) for h in range(2)]


def from_blocks(ref):
    blocks = ref.shape[1]
    return jnp.concatenate([ref[h].reshape(2 * blocks, 128) for h in range(2)], axis=1)


def ring_order(n_z, n_y):
    def hops(d):
        return min(d[0], n_z - d[0]) + min(d[1], n_y - d[1])

    return sorted(((dz, dy) for dz in range(n_z) for dy in range(n_y)), key=hops)


def kernel(
    n_ep,
    n_tp,
    tokens_h, seq_h, norm_in_h, wq_h, wk_h, wv_h, state_h, gain_h, wo_h, norm_mid_h,
    route_h, score_h, gate_h, up_h, down_h,
    out_ref,
    tokens, seq, norm_in, w_qkv, state, gain, wo, norm_mid, route, score, gate, up, down,
    carried, a_send, a_recv, b_send, rows, own, d_send, d_recv, x_send, x_recv, e_send, e_recv,
    load_sem, line_sem, a_ssem, a_rsem, b_ssem, b_rsem, g_ssem, g_rsem, f_ssem, f_rsem, d_ssem, d_rsem,
    x_ssem, x_rsem, e_ssem, e_rsem,
):
    chips = n_ep // 2
    ep = lax.axis_index("ep")
    tp = lax.axis_index("tp")
    chip = lax.div(ep, 2)
    core = lax.rem(ep, 2)
    other = 1 - core

    def peer(d):
        return lax.rem(tp + d, n_tp)

    n_y = 8 if chips % 8 == 0 else 2
    n_z = chips // n_y
    z = lax.div(chip, n_y)
    y = lax.rem(chip, n_y)
    offsets = ring_order(n_z, n_y)
    near = chips * 5 // 8

    def ahead(dz, dy):
        return lax.rem(z + dz, n_z) * n_y + lax.rem(y + dy, n_y)

    def target(p):
        return ahead(*offsets[p])

    def source(p):
        dz, dy = offsets[p]
        return ahead(n_z - dz, n_y - dy)

    def ep_id(c, co):
        return {"ep": c * 2 + co, "tp": tp}

    def tp_id(d):
        return {"ep": ep, "tp": peer(d)}

    sources = (tokens_h, seq_h, norm_in_h, wq_h, wk_h, wv_h, state_h, gain_h, wo_h, norm_mid_h,
               route_h, score_h, gate_h, up_h, down_h)
    places = (tokens, seq, norm_in, w_qkv.at[:, :128], w_qkv.at[:, 128:256], w_qkv.at[:, 256:], state, gain, wo, norm_mid, route, score, gate, up, down)
    loads = [pltpu.make_async_copy(s, p, load_sem.at[i]) for i, (s, p) in enumerate(zip(sources, places))]
    (l_tokens, l_seq, l_norm_in, l_wq, l_wk, l_wv, l_state, l_gain, l_wo, l_norm_mid, l_route, l_score,
     l_gate, l_up, l_down) = loads
    for load in (l_tokens, l_norm_in, l_seq, l_wq, l_wk, l_wv, l_route, l_score, l_state, l_gain, l_wo,
                 l_norm_mid, l_gate, l_up, l_down):
        load.start()

    barrier = pltpu.get_barrier_semaphore()

    lines = [ahead(0, d) for d in range(1, n_y)] + [ahead(d, 0) for d in range(1, n_z)]
    for d in range(1, n_tp):
        pl.semaphore_signal(barrier, inc=1, device_id=tp_id(d), device_id_type=MESH)
    pl.semaphore_signal(barrier, inc=1, device_id=ep_id(chip, other), device_id_type=MESH)
    for c in lines:
        pl.semaphore_signal(barrier, inc=1, device_id=ep_id(c, core), device_id_type=MESH)

    l_tokens.wait()
    l_norm_in.wait()
    token_f = tokens[...].astype(F32)
    normed = (
        token_f * lax.rsqrt(jnp.mean(token_f * token_f, axis=-1, keepdims=True) + EPS) * norm_in[...]
    ).astype(BF16)
    l_seq.wait()
    n_rows = token_f.shape[0]
    sub = lax.broadcasted_iota(jnp.int32, (n_rows, n_rows), 0)
    lane = lax.broadcasted_iota(jnp.int32, (n_rows, n_rows), 1)

    def column(row):
        return jnp.sum(jnp.where(sub == lane, row.astype(F32), 0.0), axis=1, keepdims=True)

    positions = column(seq[...])
    key_lane = lax.broadcasted_iota(jnp.int32, (n_rows, 128), 1)
    pair = lax.rem(key_lane, 64).astype(F32)
    angles = positions * jnp.exp(pair * (-jnp.log(10000.0) / 64.0))
    cosine = jnp.cos(angles)
    sine = jnp.where(key_lane < 64, -1.0, 1.0) * jnp.sin(angles)

    def rotate(x):
        return x * cosine + pltpu.roll(x, 64, 1) * sine

    l_wq.wait()
    l_wk.wait()
    l_wv.wait()
    projected = dot(normed, w_qkv[...]).astype(BF16).astype(F32)
    q_rot = rotate(projected[:, :128])
    k_rot = rotate(projected[:, 128:256]) * (128.0 ** -0.5)
    value_rows = projected[:, 256:]
    within = jnp.sum(q_rot * k_rot, axis=-1, keepdims=True) * value_rows
    q_cols = q_rot.T
    l_state.wait()
    for b in range(n_rows):
        carried[b : b + 1, :] = jnp.sum(q_cols[:, b : b + 1] * state[b, 0], axis=0, keepdims=True)
    head = jnp.full((1, 1), tp, jnp.int32).astype(F32)
    decay = 1.0 - jnp.exp2(-2.0 - 2.0 * head)
    retained = decay * carried[...] + within
    centred = retained - jnp.mean(retained, axis=-1, keepdims=True)
    variance = jnp.mean(centred * centred, axis=-1, keepdims=True)
    l_gain.wait()
    ret_out = (centred * lax.rsqrt(variance + EPS) * gain[...]).astype(BF16)
    l_wo.wait()
    width = out_ref.shape[1]
    mine = pl.ds(pl.multiple_of(tp * width, 128), width)

    order = [2, 1, 3]
    for d in order:
        columns = pl.ds(pl.multiple_of(peer(d) * width, 128), width)
        a_send[d] = dot(ret_out, wo[:, columns]).astype(BF16)
    own_part = dot(ret_out, wo[:, mine]).astype(BF16).astype(F32)

    pl.semaphore_wait(barrier, n_tp + len(lines))
    for d in range(1, n_z):
        pl.semaphore_signal(line_sem, inc=1, device_id=ep_id(ahead(d, 0), core), device_id_type=MESH)
    a_copies = {}
    for d in order:
        a_copies[d] = pltpu.make_async_remote_copy(
            src_ref=a_send.at[d], dst_ref=a_recv.at[d], send_sem=a_ssem.at[d], recv_sem=a_rsem.at[d],
            device_id=tp_id(d), device_id_type=MESH,
        )
        a_copies[d].start()

    l_route.wait()
    l_score.wait()
    experts = chips
    expert_lane = lax.broadcasted_iota(jnp.int32, (n_rows, 2 * experts), 1)
    choice = [column(route[k : k + 1, :]).astype(jnp.int32) for k in range(2)]
    named = [(expert_lane == c).astype(F32) for c in choice]
    earlier = dot((lane < sub).astype(BF16), (named[0] + named[1]).astype(BF16))
    picked = []
    for k in range(2):
        rank = jnp.sum(earlier * named[k], axis=1, keepdims=True).astype(jnp.int32)
        picked.append((expert_lane == choice[k] * 2 + rank).astype(F32))
    placing = (picked[0] + picked[1]).astype(BF16)
    grown = jnp.exp(score[...] - jnp.max(score[...], axis=0, keepdims=True))
    weights = grown / jnp.sum(grown, axis=0, keepdims=True)
    combine = picked[0] * column(weights[0:1, :]) + picked[1] * column(weights[1:2, :])
    combine_high, combine_low = split(combine)


    attended = own_part
    for d in (1, 3, 2):
        a_copies[d].wait_recv()
        attended = attended + a_recv[d].astype(F32)
    resid = (tokens[:, mine].astype(F32) + attended).astype(BF16)

    packed = dot_rows(placing, resid).astype(BF16)
    for h, part in enumerate(to_blocks(packed)):
        b_send[h] = part

    here = rows.at[tp, core]
    groups = (pl.ds(0, near), pl.ds(near, chips - near))
    pl.semaphore_wait(line_sem, n_z - 1)
    for p in range(chips - 1, 0, -1):
        far = target(p)
        pltpu.make_async_remote_copy(
            src_ref=b_send.at[:, far], dst_ref=here.at[:, p], send_sem=b_ssem, recv_sem=b_rsem.at[int(p >= near)],
            device_id=ep_id(far, core), device_id_type=MESH,
        ).start()
    for h in range(2):
        rows[tp, core, h, 0] = b_send[h, chip]

    def expect(group, recv_sem):
        first, size = ((1, near - 1), (near, chips - near))[group]
        block = here.at[:, pl.ds(first, size)]
        return pltpu.make_async_remote_copy(
            src_ref=block, dst_ref=block, send_sem=b_ssem, recv_sem=recv_sem, device_id=tp_id(1), device_id_type=MESH,
        )

    g_copies, f_copies = {}, {}

    def forward(g, d):
        block = rows.at[peer(n_tp - d) if d else tp, core].at[:, groups[g]]
        f_copies[g, d] = pltpu.make_async_remote_copy(
            src_ref=block, dst_ref=block, send_sem=f_ssem.at[g, d], recv_sem=f_rsem.at[g, d],
            device_id=ep_id(chip, other), device_id_type=MESH,
        )
        f_copies[g, d].start()

    def spread(g):
        expect(g, b_rsem.at[g]).wait_recv()
        block = here.at[:, groups[g]]
        for d in order:
            for side in range(g + 1):
                g_copies[g, d, side] = pltpu.make_async_remote_copy(
                    src_ref=block, dst_ref=block, send_sem=g_ssem.at[g + side, d], recv_sem=g_rsem.at[g + side, d],
                    device_id={"ep": chip * 2 + (other if side else core), "tp": peer(d)}, device_id_type=MESH,
                )
                g_copies[g, d, side].start()
        forward(g, 0)

    sums = {}

    def take(g, side, d):
        lane_group = peer(n_tp - d) if d else tp
        x = from_blocks(rows.at[lane_group, core if side == 0 else other].at[:, groups[g]]).astype(F32)
        columns = pl.ds(pl.multiple_of(lane_group * width, 128), width)
        part = jnp.sum(x * x, axis=-1, keepdims=True)
        y_rows = (x * norm_mid[:, columns]).astype(BF16)
        new = (part, dot_cols(y_rows, gate[0, :, columns]), dot_cols(y_rows, up[0, :, columns]))
        old = sums.get((g, side))
        sums[g, side] = new if old is None else tuple(m + n for m, n in zip(old, new))

    def finish(g, side):
        squares, g_sum, u_sum = sums[g, side]
        scale = lax.rsqrt(squares * (1.0 / (n_tp * width)) + EPS)
        gated = g_sum * scale
        return (gated / (1.0 + jnp.exp(-gated)) * (u_sum * scale)).astype(BF16)

    spread(0)
    l_norm_mid.wait()
    l_gate.wait()
    l_up.wait()
    take(0, 0, 0)
    spread(1)
    take(1, 0, 0)
    for d in (1, 3, 2):
        g_copies[0, d, 0].wait_recv()
        forward(0, d)
        take(0, 0, d)
    f_copies[0, 0].wait_recv()
    take(0, 1, 0)
    f_copies[1, 0].wait_recv()
    take(1, 1, 0)
    for d in (1, 3, 2):
        f_copies[0, d].wait_recv()
        take(0, 1, d)
    for d in (1, 3, 2):
        for side in range(2):
            g_copies[1, d, side].wait_recv()
            take(1, side, d)
    l_down.wait()
    d_copies, x_copies, totals = {}, {}, {}
    spans = [pl.ds(2 * part.start, 2 * part.size) for part in groups]

    def down_dot(both, d):
        columns = pl.ds(pl.multiple_of(peer(d) * width, 128), width)
        product = dot(both, down[0, :, columns])
        half = both.shape[0] // 2
        return product[:half], product[half:]

    both = jnp.concatenate([finish(1, 1), finish(1, 0)], axis=0)
    span = spans[1]
    for d in (2, 1, 3, 0):
        for side, part in enumerate(reversed(down_dot(both, d))):
            if d == 0 and side == 0:
                totals[1] = part
                continue
            x_send[side, d, span] = part.astype(BF16)
            x_copies[1, d, side] = pltpu.make_async_remote_copy(
                src_ref=x_send.at[side, d, span], dst_ref=x_recv.at[side, d, span],
                send_sem=x_ssem.at[1 + side, d], recv_sem=x_rsem.at[1 + side, d],
                device_id={"ep": chip * 2 + (other if side else core), "tp": peer(d)}, device_id_type=MESH,
            )
            x_copies[1, d, side].start()

    both = jnp.concatenate([finish(0, 1), finish(0, 0)], axis=0)
    span = spans[0]
    for d in (2, 1, 3, 0):
        theirs, ours = down_dot(both, d)
        d_send[d, span] = theirs.astype(BF16)
        d_copies[d] = pltpu.make_async_remote_copy(
            src_ref=d_send.at[d, span], dst_ref=d_recv.at[d, span], send_sem=d_ssem.at[d], recv_sem=d_rsem.at[d],
            device_id=ep_id(chip, other), device_id_type=MESH,
        )
        d_copies[d].start()
        own[d, span] = ours
    for d in order:
        d_copies[d].wait_recv()
        x_send[0, d, span] = (own[d, span] + d_recv[d, span].astype(F32)).astype(BF16)
        x_copies[0, d, 0] = pltpu.make_async_remote_copy(
            src_ref=x_send.at[0, d, span], dst_ref=x_recv.at[0, d, span],
            send_sem=x_ssem.at[0, d], recv_sem=x_rsem.at[0, d], device_id=tp_id(d), device_id_type=MESH,
        )
        x_copies[0, d, 0].start()
    d_copies[0].wait_recv()
    totals[0] = own[0, span] + d_recv[0, span].astype(F32)

    def give_back(g):
        span = spans[g]
        total = totals[g]
        for side in range(g, -1, -1):
            for d in (0, 1, 3, 2):
                if (g, d, side) in x_copies:
                    x_copies[g, d, side].wait_recv()
                    total = total + x_recv[side, d, span].astype(F32)
        for h, part in enumerate(to_blocks(total.astype(BF16))):
            e_send[h, groups[g]] = part
        for p in range(groups[g].start + groups[g].size - 1, max(0, groups[g].start - 1), -1):
            pltpu.make_async_remote_copy(
                src_ref=e_send.at[:, p], dst_ref=e_recv.at[:, chip], send_sem=e_ssem, recv_sem=e_rsem,
                device_id=ep_id(source(p), core), device_id_type=MESH,
            ).start()

    give_back(1)
    give_back(0)
    for h in range(2):
        e_recv[h, chip] = e_send[h, 0]
    rest = pl.ds(1, chips - 1)
    all_back = pltpu.make_async_remote_copy(
        src_ref=e_send.at[:, rest], dst_ref=e_recv.at[:, rest], send_sem=e_ssem, recv_sem=e_rsem,
        device_id=tp_id(1), device_id_type=MESH,
    )
    all_back.wait_recv()
    back = from_blocks(e_recv)
    mix = dot(combine_high, back) + dot(combine_low, back)
    out_ref[...] = (resid.astype(F32) + mix).astype(BF16)

    pltpu.make_async_remote_copy(
        src_ref=b_send.at[:, rest], dst_ref=here.at[:, rest], send_sem=b_ssem, recv_sem=b_rsem.at[0],
        device_id=tp_id(1), device_id_type=MESH,
    ).wait_send()
    all_back.wait_send()
    for d in order:
        a_copies[d].wait_send()
    for copies in (g_copies, f_copies, d_copies, x_copies):
        for copy in copies.values():
            copy.wait_send()


def body(
    n_ep, n_tp, tokens, seq_length, ret_state, norm_in, w_query, w_key, w_value, head_gain, w_output,
    norm_mid, route_expert, route_score, expert_gate, expert_up, expert_down,
):
    n_rows, model = tokens.shape
    chips = n_ep // 2
    width = model // n_tp
    args = (
        tokens, seq_length.reshape(1, -1), norm_in.reshape(1, -1), w_query, w_key, w_value, ret_state,
        head_gain.reshape(1, -1), w_output, norm_mid.reshape(1, -1), route_expert.T, route_score.T,
        expert_gate.swapaxes(1, 2), expert_up.swapaxes(1, 2), expert_down,
    )
    dma = pltpu.SemaphoreType.DMA
    blocks = (2, chips, 2, width // 2)
    held = [jax.ShapeDtypeStruct((model, 512), BF16) if a is w_query else a for a in args if a is not w_key and a is not w_value]
    scratch = [pltpu.VMEM(a.shape, a.dtype) for a in held] + [
        pltpu.VMEM((n_rows, head_gain.shape[0]), F32),
        pltpu.VMEM((n_tp, n_rows, width), BF16),
        pltpu.VMEM((n_tp, n_rows, width), BF16),
        pltpu.VMEM(blocks, BF16),
        pltpu.VMEM((n_tp, 2) + blocks, BF16),
        pltpu.VMEM((n_tp, 2 * chips, width), F32),
        pltpu.VMEM((n_tp, 2 * chips, width), BF16),
        pltpu.VMEM((n_tp, 2 * chips, width), BF16),
        pltpu.VMEM((2, n_tp, 2 * chips, width), BF16),
        pltpu.VMEM((2, n_tp, 2 * chips, width), BF16),
        pltpu.VMEM(blocks, BF16),
        pltpu.VMEM(blocks, BF16),
        dma((len(args),)),
        pltpu.SemaphoreType.REGULAR,
        dma((n_tp,)), dma((n_tp,)),
        dma, dma((2,)),
        dma((3, n_tp)), dma((3, n_tp)),
        dma((2, n_tp)), dma((2, n_tp)),
        dma((n_tp,)), dma((n_tp,)),
        dma((3, n_tp)), dma((3, n_tp)),
        dma, dma,
    ]
    return pl.pallas_call(
        functools.partial(kernel, n_ep, n_tp),
        out_shape=jax.ShapeDtypeStruct((n_rows, width), BF16),
        in_specs=[pl.BlockSpec(memory_space=pl.ANY)] * len(args),
        out_specs=pl.BlockSpec(memory_space=pltpu.VMEM),
        scratch_shapes=scratch,
        compiler_params=pltpu.CompilerParams(collective_id=0, has_side_effects=True),
        name="step",
    )(*args)


def solution(mesh):
    placed = (
        P("ep", None),
        P("ep"),
        P("ep", "tp", None, None),
        P(),
        P(None, "tp"),
        P(None, "tp"),
        P(None, "tp"),
        P("tp"),
        P("tp", None),
        P(),
        P("ep", None),
        P("ep", None),
        P("ep", None, "tp"),
        P("ep", None, "tp"),
        P("ep", "tp", None),
    )
    step = functools.partial(body, mesh.shape["ep"], mesh.shape["tp"])
    return jax.shard_map(step, mesh=mesh, in_specs=placed, out_specs=P("ep", "tp"), check_vma=False)
```

time: 57.5 us -> 46.8 us (0.81)
  local copies, waits for them, and re-layouts: 7.65 us -> 1.3 us
  Pallas kernels: 49.6 us -> 45.3 us
    unnamed x7 -> x1, local copies, waits for them, and re-layouts: 7.65 us -> 1.3 us
    pallas_call x1, Pallas kernels: 49.6 us -> 45.3 us  [body(): pl.pallas_call(functools.partial(kernel, n_ep, n_tp), out_shape=jax.Shape...]
where the time goes in v2:
time: 46.8 us; the launch traced here: 46.6 us
  Pallas kernels  45.3 us (97%)
  local copies, waits for them, and re-layouts  1.3 us (3%)
    pallas_call x1, Pallas kernels, body(): pl.pallas_call(functools.partial(kernel, n_ep, n_tp), out_shape=jax.Shape...  45.3 us
    unnamed x1, local copies, waits for them, and re-layouts  1.3 us

profile of v2, /device:TPU:1, one launch (start us, length us, event | category | flops | bytes accessed | tf_op | source)
XLA Modules:
  0.0 46.6 jit_solution(17999598861234081809)
XLA Ops:
  0.0 45.3 %step.1 = bf16[16,256]{1,0:T(8,128)(2,1)} custom-call(bf16[16,1024]{1,0:T(8,128)(2,1)} %tokens_h.1, s32[1,16]{1,0:T(1,128)} %bitcast.15, f32[1,1024]{1,0:T(1,128)} %bitcast.10, bf16[1024,128]{1,0:T(8,128)(2,1)} %wq_h.1, bf16[1024,128]{1,0:T(8,128)(2,1)} %wk_h.1, bf16[1024,256]{1,0:T(8,128)(2,1)} %wv_h.1, f32[16,1,128,256]{3,2,1,0:T(8,128)} %state_h.1, ...), custom_call_target="tpu_custom_call" | custom-call | tf_op jit(solution)/shard_map/step/pallas_call | solution.py:413
  45.4 1.3 %copy.17 = bf16[16,256]{1,0:T(8,128)(2,1)} copy(bf16[16,256]{1,0:T(8,128)(2,1)} %step.1) | data formatting | bytes 16384

commit v3 on v2

--- a/solution.py
+++ b/solution.py
@@ -95,10 +95,13 @@
                route_h, score_h, gate_h, up_h, down_h)
     places = (tokens, seq, norm_in, w_qkv.at[:, :128], w_qkv.at[:, 128:256], w_qkv.at[:, 256:], state, gain, wo, norm_mid, route, score, gate, up, down)
     loads = [pltpu.make_async_copy(s, p, load_sem.at[i]) for i, (s, p) in enumerate(zip(sources, places))]
+    halves = [pl.ds(0, tokens.shape[0] // 2), pl.ds(tokens.shape[0] // 2, tokens.shape[0] // 2)]
+    l_states = [
+        pltpu.make_async_copy(state_h.at[half], state.at[half], load_sem.at[len(loads) + i]) for i, half in enumerate(halves)
+    ]
     (l_tokens, l_seq, l_norm_in, l_wq, l_wk, l_wv, l_state, l_gain, l_wo, l_norm_mid, l_route, l_score,
      l_gate, l_up, l_down) = loads
-    for load in (l_tokens, l_norm_in, l_seq, l_wq, l_wk, l_wv, l_route, l_score, l_state, l_gain, l_wo,
-                 l_norm_mid, l_gate, l_up, l_down):
+    for load in (l_tokens, l_norm_in, l_seq, l_wq, l_wk, l_wv):
         load.start()
 
     barrier = pltpu.get_barrier_semaphore()
@@ -110,13 +113,16 @@
     for c in lines:
         pl.semaphore_signal(barrier, inc=1, device_id=ep_id(c, core), device_id_type=MESH)
 
+    for load in (*l_states, l_gain, l_wo):
+        load.start()
     l_tokens.wait()
     l_norm_in.wait()
+    l_seq.wait()
+    l_wq.wait()
+    l_wk.wait()
+    l_wv.wait()
     token_f = tokens[...].astype(F32)
-    normed = (
-        token_f * lax.rsqrt(jnp.mean(token_f * token_f, axis=-1, keepdims=True) + EPS) * norm_in[...]
-    ).astype(BF16)
-    l_seq.wait()
+    row_scale = lax.rsqrt(jnp.mean(token_f * token_f, axis=-1, keepdims=True) + EPS)
     n_rows = token_f.shape[0]
     sub = lax.broadcasted_iota(jnp.int32, (n_rows, n_rows), 0)
     lane = lax.broadcasted_iota(jnp.int32, (n_rows, n_rows), 1)
@@ -134,17 +140,17 @@
     def rotate(x):
         return x * cosine + pltpu.roll(x, 64, 1) * sine
 
-    l_wq.wait()
-    l_wk.wait()
-    l_wv.wait()
-    projected = dot(normed, w_qkv[...]).astype(BF16).astype(F32)
+    projected = dot((token_f * norm_in[...]).astype(BF16), w_qkv[...]) * row_scale
     q_rot = rotate(projected[:, :128])
     k_rot = rotate(projected[:, 128:256]) * (128.0 ** -0.5)
     value_rows = projected[:, 256:]
     within = jnp.sum(q_rot * k_rot, axis=-1, keepdims=True) * value_rows
+    for load in (l_route, l_score, l_norm_mid, l_gate, l_up, l_down):
+        load.start()
     q_cols = q_rot.T
-    l_state.wait()
     for b in range(n_rows):
+        if b % (n_rows // 2) == 0:
+            l_states[b // (n_rows // 2)].wait()
         carried[b : b + 1, :] = jnp.sum(q_cols[:, b : b + 1] * state[b, 0], axis=0, keepdims=True)
     head = jnp.full((1, 1), tp, jnp.int32).astype(F32)
     decay = 1.0 - jnp.exp2(-2.0 - 2.0 * head)
@@ -243,20 +249,18 @@
                 g_copies[g, d, side].start()
         forward(g, 0)
 
-    sums = {}
-
-    def take(g, side, d):
+    def take(blocks, d, old):
         lane_group = peer(n_tp - d) if d else tp
-        x = from_blocks(rows.at[lane_group, core if side == 0 else other].at[:, groups[g]]).astype(F32)
+        parts = [from_blocks(rows.at[lane_group, other if side else core].at[:, groups[g]]) for g, side in blocks]
+        x = (parts[0] if len(parts) == 1 else jnp.concatenate(parts, axis=0)).astype(F32)
         columns = pl.ds(pl.multiple_of(lane_group * width, 128), width)
         part = jnp.sum(x * x, axis=-1, keepdims=True)
         y_rows = (x * norm_mid[:, columns]).astype(BF16)
         new = (part, dot_cols(y_rows, gate[0, :, columns]), dot_cols(y_rows, up[0, :, columns]))
-        old = sums.get((g, side))
-        sums[g, side] = new if old is None else tuple(m + n for m, n in zip(old, new))
-
-    def finish(g, side):
-        squares, g_sum, u_sum = sums[g, side]
+        return new if old is None else tuple(m + n for m, n in zip(old, new))
+
+    def finish(sums):
+        squares, g_sum, u_sum = sums
         scale = lax.rsqrt(squares * (1.0 / (n_tp * width)) + EPS)
         gated = g_sum * scale
         return (gated / (1.0 + jnp.exp(-gated)) * (u_sum * scale)).astype(BF16)
@@ -265,79 +269,67 @@
     l_norm_mid.wait()
     l_gate.wait()
     l_up.wait()
-    take(0, 0, 0)
+    first = take([(0, 0)], 0, None)
     spread(1)
-    take(1, 0, 0)
+    f_copies[0, 0].wait_recv()
+    f_copies[1, 0].wait_recv()
+    others = take([(0, 1), (1, 1), (1, 0)], 0, None)
     for d in (1, 3, 2):
         g_copies[0, d, 0].wait_recv()
         forward(0, d)
-        take(0, 0, d)
-    f_copies[0, 0].wait_recv()
-    take(0, 1, 0)
-    f_copies[1, 0].wait_recv()
-    take(1, 1, 0)
+        first = take([(0, 0)], d, first)
     for d in (1, 3, 2):
+        g_copies[1, d, 0].wait_recv()
+        g_copies[1, d, 1].wait_recv()
         f_copies[0, d].wait_recv()
-        take(0, 1, d)
-    for d in (1, 3, 2):
-        for side in range(2):
-            g_copies[1, d, side].wait_recv()
-            take(1, side, d)
+        others = take([(0, 1), (1, 1), (1, 0)], d, others)
     l_down.wait()
     d_copies, x_copies, totals = {}, {}, {}
-    spans = [pl.ds(2 * part.start, 2 * part.size) for part in groups]
-
-    def down_dot(both, d):
-        columns = pl.ds(pl.multiple_of(peer(d) * width, 128), width)
-        product = dot(both, down[0, :, columns])
-        half = both.shape[0] // 2
-        return product[:half], product[half:]
-
-    both = jnp.concatenate([finish(1, 1), finish(1, 0)], axis=0)
-    span = spans[1]
+
+    hidden = jnp.concatenate([finish(others), finish(first)], axis=0)
+    n_near, n_far = 2 * near, 2 * (chips - near)
+    near_span, far_span = pl.ds(0, n_near), pl.ds(n_near, n_far)
+    def quarter(d):
+        return dot(hidden, down[0, :, pl.ds(pl.multiple_of(peer(d) * width, 128), width)])
+
+    n_all = n_near + n_far
+    products = {d: quarter(d) for d in (2, 1)}
     for d in (2, 1, 3, 0):
-        for side, part in enumerate(reversed(down_dot(both, d))):
-            if d == 0 and side == 0:
-                totals[1] = part
-                continue
-            x_send[side, d, span] = part.astype(BF16)
-            x_copies[1, d, side] = pltpu.make_async_remote_copy(
-                src_ref=x_send.at[side, d, span], dst_ref=x_recv.at[side, d, span],
-                send_sem=x_ssem.at[1 + side, d], recv_sem=x_rsem.at[1 + side, d],
-                device_id={"ep": chip * 2 + (other if side else core), "tp": peer(d)}, device_id_type=MESH,
-            )
-            x_copies[1, d, side].start()
-
-    both = jnp.concatenate([finish(0, 1), finish(0, 0)], axis=0)
-    span = spans[0]
-    for d in (2, 1, 3, 0):
-        theirs, ours = down_dot(both, d)
-        d_send[d, span] = theirs.astype(BF16)
+        if d == 3:
+            products.update({each: quarter(each) for each in (3, 0)})
+        product = products[d]
+        d_send[d] = product[:n_all].astype(BF16)
         d_copies[d] = pltpu.make_async_remote_copy(
-            src_ref=d_send.at[d, span], dst_ref=d_recv.at[d, span], send_sem=d_ssem.at[d], recv_sem=d_rsem.at[d],
+            src_ref=d_send.at[d], dst_ref=d_recv.at[d], send_sem=d_ssem.at[d], recv_sem=d_rsem.at[d],
             device_id=ep_id(chip, other), device_id_type=MESH,
         )
         d_copies[d].start()
-        own[d, span] = ours
+        own[d, far_span] = product[n_all : n_all + n_far]
+        own[d, near_span] = product[n_all + n_far :]
+
+    def across(g, d, span):
+        x_send[d, span] = (own[d, span] + d_recv[d, span].astype(F32)).astype(BF16)
+        x_copies[g, d] = pltpu.make_async_remote_copy(
+            src_ref=x_send.at[d, span], dst_ref=x_recv.at[d, span],
+            send_sem=x_ssem.at[g, d], recv_sem=x_rsem.at[g, d], device_id=tp_id(d), device_id_type=MESH,
+        )
+        x_copies[g, d].start()
+
     for d in order:
         d_copies[d].wait_recv()
-        x_send[0, d, span] = (own[d, span] + d_recv[d, span].astype(F32)).astype(BF16)
-        x_copies[0, d, 0] = pltpu.make_async_remote_copy(
-            src_ref=x_send.at[0, d, span], dst_ref=x_recv.at[0, d, span],
-            send_sem=x_ssem.at[0, d], recv_sem=x_rsem.at[0, d], device_id=tp_id(d), device_id_type=MESH,
-        )
-        x_copies[0, d, 0].start()
+        across(1, d, far_span)
+    for d in order:
+        across(0, d, near_span)
     d_copies[0].wait_recv()
-    totals[0] = own[0, span] + d_recv[0, span].astype(F32)
+    for g, span in enumerate((near_span, far_span)):
+        totals[g] = own[0, span] + d_recv[0, span].astype(F32)
 
     def give_back(g):
-        span = spans[g]
+        span = (near_span, far_span)[g]
         total = totals[g]
-        for side in range(g, -1, -1):
-            for d in (0, 1, 3, 2):
-                if (g, d, side) in x_copies:
-                    x_copies[g, d, side].wait_recv()
-                    total = total + x_recv[side, d, span].astype(F32)
+        for d in (1, 3, 2):
+            x_copies[g, d].wait_recv()
+            total = total + x_recv[d, span].astype(F32)
         for h, part in enumerate(to_blocks(total.astype(BF16))):
             e_send[h, groups[g]] = part
         for p in range(groups[g].start + groups[g].size - 1, max(0, groups[g].start - 1), -1):
@@ -396,18 +388,18 @@
         pltpu.VMEM((n_tp, 2 * chips, width), F32),
         pltpu.VMEM((n_tp, 2 * chips, width), BF16),
         pltpu.VMEM((n_tp, 2 * chips, width), BF16),
-        pltpu.VMEM((2, n_tp, 2 * chips, width), BF16),
-        pltpu.VMEM((2, n_tp, 2 * chips, width), BF16),
+        pltpu.VMEM((n_tp, 2 * chips, width), BF16),
+        pltpu.VMEM((n_tp, 2 * chips, width), BF16),
         pltpu.VMEM(blocks, BF16),
         pltpu.VMEM(blocks, BF16),
-        dma((len(args),)),
+        dma((len(args) + 2,)),
         pltpu.SemaphoreType.REGULAR,
         dma((n_tp,)), dma((n_tp,)),
         dma, dma((2,)),
         dma((3, n_tp)), dma((3, n_tp)),
         dma((2, n_tp)), dma((2, n_tp)),
         dma((n_tp,)), dma((n_tp,)),
-        dma((3, n_tp)), dma((3, n_tp)),
+        dma((2, n_tp)), dma((2, n_tp)),
         dma, dma,
     ]
     return pl.pallas_call(
@@ -416,9 +408,9 @@
         in_specs=[pl.BlockSpec(memory_space=pl.ANY)] * len(args),
         out_specs=pl.BlockSpec(memory_space=pltpu.VMEM),
         scratch_shapes=scratch,
-        compiler_params=pltpu.CompilerParams(collective_id=0, has_side_effects=True),
+        compiler_params=pltpu.CompilerParams(collective_id=0, has_side_effects=True, vmem_limit_bytes=40 << 20),
         name="step",
-    )(*args)
+    )(*[pltpu.with_memory_space_constraint(a, pltpu.HBM) for a in args])
 
 
 def solution(mesh):

time: 46.8 us -> 43.6 us (0.932)
  Pallas kernels: 45.3 us -> 42.9 us
  local copies, waits for them, and re-layouts: 1.3 us -> 0.6 us
    pallas_call x1, Pallas kernels: 45.3 us -> 42.9 us  [body(): pl.pallas_call(functools.partial(kernel, n_ep, n_tp), out_shape=jax.Shape...]
    unnamed x1, local copies, waits for them, and re-layouts: 1.3 us -> 0.6 us
where the time goes in v3:
time: 43.6 us; the launch traced here: 43.5 us
  Pallas kernels  42.9 us (98%)
  local copies, waits for them, and re-layouts  0.6 us (1%)
    pallas_call x1, Pallas kernels, body(): pl.pallas_call(functools.partial(kernel, n_ep, n_tp), out_shape=jax.Shape...  42.9 us

profile of v3, /device:TPU:1, one launch (start us, length us, event | category | flops | bytes accessed | tf_op | source)
XLA Modules:
  0.0 43.5 jit_solution(2496729223837548444)
XLA Ops:
  0.0 42.9 %step.1 = bf16[16,256]{1,0:T(8,128)(2,1)S(1)} custom-call(bf16[16,1024]{1,0:T(8,128)(2,1)} %tokens_h.1, s32[1,16]{1,0:T(1,128)} %bitcast.15, f32[1,1024]{1,0:T(1,128)} %bitcast.10, bf16[1024,128]{1,0:T(8,128)(2,1)} %wq_h.1, bf16[1024,128]{1,0:T(8,128)(2,1)} %wk_h.1, bf16[1024,256]{1,0:T(8,128)(2,1)} %wv_h.1, f32[16,1,128,256]{3,2,1,0:T(8,128)} %state_h.1, ...), custom_call_target="tpu_custom_call" | custom-call | tf_op jit(solution)/shard_map/step/pallas_call | solution.py:405
  42.9 0.6 %copy.17 = bf16[16,256]{1,0:T(8,128)(2,1)} copy(bf16[16,256]{1,0:T(8,128)(2,1)S(1)} %step.1) | data formatting | bytes 16384

commit v4 on v3

--- a/solution.py
+++ b/solution.py
@@ -36,8 +36,8 @@
 
 
 def from_blocks(ref):
-    blocks = ref.shape[1]
-    return jnp.concatenate([ref[h].reshape(2 * blocks, 128) for h in range(2)], axis=1)
+    blocks = ref.shape[0]
+    return jnp.concatenate([ref[:, h].reshape(2 * blocks, 128) for h in range(2)], axis=1)
 
 
 def ring_order(n_z, n_y):
@@ -53,7 +53,7 @@
     tokens_h, seq_h, norm_in_h, wq_h, wk_h, wv_h, state_h, gain_h, wo_h, norm_mid_h,
     route_h, score_h, gate_h, up_h, down_h,
     out_ref,
-    tokens, seq, norm_in, w_qkv, state, gain, wo, norm_mid, route, score, gate, up, down,
+    tokens, seq, norm_in, w_qkv, state, gain, wo, norm_mid, route, score, gate_up, down,
     carried, a_send, a_recv, b_send, rows, own, d_send, d_recv, x_send, x_recv, e_send, e_recv,
     load_sem, line_sem, a_ssem, a_rsem, b_ssem, b_rsem, g_ssem, g_rsem, f_ssem, f_rsem, d_ssem, d_rsem,
     x_ssem, x_rsem, e_ssem, e_rsem,
@@ -93,34 +93,37 @@
 
     sources = (tokens_h, seq_h, norm_in_h, wq_h, wk_h, wv_h, state_h, gain_h, wo_h, norm_mid_h,
                route_h, score_h, gate_h, up_h, down_h)
-    places = (tokens, seq, norm_in, w_qkv.at[:, :128], w_qkv.at[:, 128:256], w_qkv.at[:, 256:], state, gain, wo, norm_mid, route, score, gate, up, down)
-    loads = [pltpu.make_async_copy(s, p, load_sem.at[i]) for i, (s, p) in enumerate(zip(sources, places))]
-    halves = [pl.ds(0, tokens.shape[0] // 2), pl.ds(tokens.shape[0] // 2, tokens.shape[0] // 2)]
+    places = (tokens, seq, norm_in, w_qkv.at[:, :128], w_qkv.at[:, 128:256], w_qkv.at[:, 256:], state, gain, wo, norm_mid, route, score, gate_up.at[pl.ds(0, 1)], gate_up.at[pl.ds(1, 1)], down)
+    def load(i, sem):
+        return pltpu.make_async_copy(sources[i], places[i], load_sem.at[sem])
+
+    l_tokens, l_seq, l_norm_in, l_wq, l_wk, l_wv = [load(i, sem) for i, sem in enumerate((0, 1, 2, 3, 3, 3))]
+    l_gain, l_wo, l_norm_mid, l_route, l_score = [load(i, sem) for i, sem in ((7, 6), (8, 7), (9, 0), (10, 1), (11, 2))]
+    l_gate, l_up, l_down = load(12, 3), load(13, 3), load(14, 4)
+    l_qkv = pltpu.make_async_copy(w_qkv, w_qkv, load_sem.at[3])
+    l_gate_up = pltpu.make_async_copy(gate_up, gate_up, load_sem.at[3])
+    n_half = tokens.shape[0] // 2
     l_states = [
-        pltpu.make_async_copy(state_h.at[half], state.at[half], load_sem.at[len(loads) + i]) for i, half in enumerate(halves)
+        pltpu.make_async_copy(state_h.at[half], state.at[half], load_sem.at[4 + i])
+        for i, half in enumerate((pl.ds(0, n_half), pl.ds(n_half, n_half)))
     ]
-    (l_tokens, l_seq, l_norm_in, l_wq, l_wk, l_wv, l_state, l_gain, l_wo, l_norm_mid, l_route, l_score,
-     l_gate, l_up, l_down) = loads
-    for load in (l_tokens, l_norm_in, l_seq, l_wq, l_wk, l_wv):
-        load.start()
+    for each in (l_tokens, l_norm_in, l_seq, l_wq, l_wk, l_wv):
+        each.start()
 
     barrier = pltpu.get_barrier_semaphore()
 
     lines = [ahead(0, d) for d in range(1, n_y)] + [ahead(d, 0) for d in range(1, n_z)]
+    for c in lines:
+        pl.semaphore_signal(barrier, inc=1, device_id=ep_id(c, core), device_id_type=MESH)
     for d in range(1, n_tp):
         pl.semaphore_signal(barrier, inc=1, device_id=tp_id(d), device_id_type=MESH)
     pl.semaphore_signal(barrier, inc=1, device_id=ep_id(chip, other), device_id_type=MESH)
-    for c in lines:
-        pl.semaphore_signal(barrier, inc=1, device_id=ep_id(c, core), device_id_type=MESH)
-
-    for load in (*l_states, l_gain, l_wo):
-        load.start()
+
+    for each in (*l_states, l_gain, l_wo):
+        each.start()
     l_tokens.wait()
     l_norm_in.wait()
     l_seq.wait()
-    l_wq.wait()
-    l_wk.wait()
-    l_wv.wait()
     token_f = tokens[...].astype(F32)
     row_scale = lax.rsqrt(jnp.mean(token_f * token_f, axis=-1, keepdims=True) + EPS)
     n_rows = token_f.shape[0]
@@ -140,18 +143,20 @@
     def rotate(x):
         return x * cosine + pltpu.roll(x, 64, 1) * sine
 
-    projected = dot((token_f * norm_in[...]).astype(BF16), w_qkv[...]) * row_scale
+    gained = (token_f * norm_in[...]).astype(BF16)
+    l_qkv.wait()
+    projected = dot(gained, w_qkv[...]) * row_scale
     q_rot = rotate(projected[:, :128])
     k_rot = rotate(projected[:, 128:256]) * (128.0 ** -0.5)
     value_rows = projected[:, 256:]
     within = jnp.sum(q_rot * k_rot, axis=-1, keepdims=True) * value_rows
-    for load in (l_route, l_score, l_norm_mid, l_gate, l_up, l_down):
-        load.start()
     q_cols = q_rot.T
     for b in range(n_rows):
         if b % (n_rows // 2) == 0:
             l_states[b // (n_rows // 2)].wait()
         carried[b : b + 1, :] = jnp.sum(q_cols[:, b : b + 1] * state[b, 0], axis=0, keepdims=True)
+    for each in (l_route, l_score, l_norm_mid, l_gate, l_up, l_down):
+        each.start()
     head = jnp.full((1, 1), tp, jnp.int32).astype(F32)
     decay = 1.0 - jnp.exp2(-2.0 - 2.0 * head)
     retained = decay * carried[...] + within
@@ -175,7 +180,7 @@
     a_copies = {}
     for d in order:
         a_copies[d] = pltpu.make_async_remote_copy(
-            src_ref=a_send.at[d], dst_ref=a_recv.at[d], send_sem=a_ssem.at[d], recv_sem=a_rsem.at[d],
+            src_ref=a_send.at[d], dst_ref=a_recv.at[d], send_sem=a_ssem, recv_sem=a_rsem,
             device_id=tp_id(d), device_id_type=MESH,
         )
         a_copies[d].start()
@@ -199,14 +204,18 @@
 
 
     attended = own_part
+    a_all = pltpu.make_async_remote_copy(
+        src_ref=a_send.at[pl.ds(1, n_tp - 1)], dst_ref=a_recv.at[pl.ds(1, n_tp - 1)], send_sem=a_ssem, recv_sem=a_rsem,
+        device_id=tp_id(1), device_id_type=MESH,
+    )
+    a_all.wait_recv()
     for d in (1, 3, 2):
-        a_copies[d].wait_recv()
         attended = attended + a_recv[d].astype(F32)
     resid = (tokens[:, mine].astype(F32) + attended).astype(BF16)
 
     packed = dot_rows(placing, resid).astype(BF16)
     for h, part in enumerate(to_blocks(packed)):
-        b_send[h] = part
+        b_send[:, h] = part
 
     here = rows.at[tp, core]
     groups = (pl.ds(0, near), pl.ds(near, chips - near))
@@ -214,15 +223,14 @@
     for p in range(chips - 1, 0, -1):
         far = target(p)
         pltpu.make_async_remote_copy(
-            src_ref=b_send.at[:, far], dst_ref=here.at[:, p], send_sem=b_ssem, recv_sem=b_rsem.at[int(p >= near)],
+            src_ref=b_send.at[far], dst_ref=here.at[p], send_sem=b_ssem, recv_sem=b_rsem.at[int(p >= near)],
             device_id=ep_id(far, core), device_id_type=MESH,
         ).start()
-    for h in range(2):
-        rows[tp, core, h, 0] = b_send[h, chip]
+    rows[tp, core, 0] = b_send[chip]
 
     def expect(group, recv_sem):
         first, size = ((1, near - 1), (near, chips - near))[group]
-        block = here.at[:, pl.ds(first, size)]
+        block = here.at[pl.ds(first, size)]
         return pltpu.make_async_remote_copy(
             src_ref=block, dst_ref=block, send_sem=b_ssem, recv_sem=recv_sem, device_id=tp_id(1), device_id_type=MESH,
         )
@@ -230,20 +238,20 @@
     g_copies, f_copies = {}, {}
 
     def forward(g, d):
-        block = rows.at[peer(n_tp - d) if d else tp, core].at[:, groups[g]]
+        block = rows.at[peer(n_tp - d) if d else tp, core].at[groups[g]]
         f_copies[g, d] = pltpu.make_async_remote_copy(
-            src_ref=block, dst_ref=block, send_sem=f_ssem.at[g, d], recv_sem=f_rsem.at[g, d],
+            src_ref=block, dst_ref=block, send_sem=f_ssem.at[g], recv_sem=f_rsem.at[n_tp * g + d],
             device_id=ep_id(chip, other), device_id_type=MESH,
         )
         f_copies[g, d].start()
 
     def spread(g):
         expect(g, b_rsem.at[g]).wait_recv()
-        block = here.at[:, groups[g]]
+        block = here.at[groups[g]]
         for d in order:
             for side in range(g + 1):
                 g_copies[g, d, side] = pltpu.make_async_remote_copy(
-                    src_ref=block, dst_ref=block, send_sem=g_ssem.at[g + side, d], recv_sem=g_rsem.at[g + side, d],
+                    src_ref=block, dst_ref=block, send_sem=g_ssem.at[g], recv_sem=g_rsem.at[g, d],
                     device_id={"ep": chip * 2 + (other if side else core), "tp": peer(d)}, device_id_type=MESH,
                 )
                 g_copies[g, d, side].start()
@@ -251,12 +259,12 @@
 
     def take(blocks, d, old):
         lane_group = peer(n_tp - d) if d else tp
-        parts = [from_blocks(rows.at[lane_group, other if side else core].at[:, groups[g]]) for g, side in blocks]
+        parts = [from_blocks(rows.at[lane_group, other if side else core].at[groups[g]]) for g, side in blocks]
         x = (parts[0] if len(parts) == 1 else jnp.concatenate(parts, axis=0)).astype(F32)
         columns = pl.ds(pl.multiple_of(lane_group * width, 128), width)
         part = jnp.sum(x * x, axis=-1, keepdims=True)
         y_rows = (x * norm_mid[:, columns]).astype(BF16)
-        new = (part, dot_cols(y_rows, gate[0, :, columns]), dot_cols(y_rows, up[0, :, columns]))
+        new = (part, dot_cols(y_rows, gate_up[0, :, columns]), dot_cols(y_rows, gate_up[1, :, columns]))
         return new if old is None else tuple(m + n for m, n in zip(old, new))
 
     def finish(sums):
@@ -267,8 +275,7 @@
 
     spread(0)
     l_norm_mid.wait()
-    l_gate.wait()
-    l_up.wait()
+    l_gate_up.wait()
     first = take([(0, 0)], 0, None)
     spread(1)
     f_copies[0, 0].wait_recv()
@@ -279,12 +286,14 @@
         forward(0, d)
         first = take([(0, 0)], d, first)
     for d in (1, 3, 2):
-        g_copies[1, d, 0].wait_recv()
-        g_copies[1, d, 1].wait_recv()
+        block = rows.at[peer(n_tp - d), :, groups[1]]
+        pltpu.make_async_remote_copy(
+            src_ref=block, dst_ref=block, send_sem=g_ssem.at[1], recv_sem=g_rsem.at[1, d], device_id=tp_id(d), device_id_type=MESH,
+        ).wait_recv()
         f_copies[0, d].wait_recv()
         others = take([(0, 1), (1, 1), (1, 0)], d, others)
     l_down.wait()
-    d_copies, x_copies, totals = {}, {}, {}
+    d_copies, x_copies = {}, {}
 
     hidden = jnp.concatenate([finish(others), finish(first)], axis=0)
     n_near, n_far = 2 * near, 2 * (chips - near)
@@ -300,7 +309,7 @@
         product = products[d]
         d_send[d] = product[:n_all].astype(BF16)
         d_copies[d] = pltpu.make_async_remote_copy(
-            src_ref=d_send.at[d], dst_ref=d_recv.at[d], send_sem=d_ssem.at[d], recv_sem=d_rsem.at[d],
+            src_ref=d_send.at[d], dst_ref=d_recv.at[d], send_sem=d_ssem, recv_sem=d_rsem.at[d],
             device_id=ep_id(chip, other), device_id_type=MESH,
         )
         d_copies[d].start()
@@ -311,40 +320,44 @@
         x_send[d, span] = (own[d, span] + d_recv[d, span].astype(F32)).astype(BF16)
         x_copies[g, d] = pltpu.make_async_remote_copy(
             src_ref=x_send.at[d, span], dst_ref=x_recv.at[d, span],
-            send_sem=x_ssem.at[g, d], recv_sem=x_rsem.at[g, d], device_id=tp_id(d), device_id_type=MESH,
+            send_sem=x_ssem, recv_sem=x_rsem.at[g], device_id=tp_id(d), device_id_type=MESH,
         )
         x_copies[g, d].start()
 
+    cuts = (0, 3 * chips // 8, 3 * chips // 4, chips)
+    returns = [pl.ds(low, high - low) for low, high in zip(cuts, cuts[1:])]
+    spans = [pl.ds(2 * part.start, 2 * part.size) for part in returns]
     for d in order:
         d_copies[d].wait_recv()
-        across(1, d, far_span)
-    for d in order:
-        across(0, d, near_span)
+        across(2, d, spans[2])
+    for g in (1, 0):
+        for d in order:
+            across(g, d, spans[g])
     d_copies[0].wait_recv()
-    for g, span in enumerate((near_span, far_span)):
-        totals[g] = own[0, span] + d_recv[0, span].astype(F32)
 
     def give_back(g):
-        span = (near_span, far_span)[g]
-        total = totals[g]
+        span, group = spans[g], returns[g]
+        total = own[0, span] + d_recv[0, span].astype(F32)
+        others_here = x_recv.at[pl.ds(1, n_tp - 1), span]
+        pltpu.make_async_remote_copy(
+            src_ref=others_here, dst_ref=others_here, send_sem=x_ssem, recv_sem=x_rsem.at[g], device_id=tp_id(1), device_id_type=MESH,
+        ).wait_recv()
         for d in (1, 3, 2):
-            x_copies[g, d].wait_recv()
             total = total + x_recv[d, span].astype(F32)
         for h, part in enumerate(to_blocks(total.astype(BF16))):
-            e_send[h, groups[g]] = part
-        for p in range(groups[g].start + groups[g].size - 1, max(0, groups[g].start - 1), -1):
+            e_send[group, h] = part
+        for p in range(group.start + group.size - 1, max(0, group.start - 1), -1):
             pltpu.make_async_remote_copy(
-                src_ref=e_send.at[:, p], dst_ref=e_recv.at[:, chip], send_sem=e_ssem, recv_sem=e_rsem,
+                src_ref=e_send.at[p], dst_ref=e_recv.at[chip], send_sem=e_ssem, recv_sem=e_rsem,
                 device_id=ep_id(source(p), core), device_id_type=MESH,
             ).start()
 
-    give_back(1)
-    give_back(0)
-    for h in range(2):
-        e_recv[h, chip] = e_send[h, 0]
+    for g in (2, 1, 0):
+        give_back(g)
+    e_recv[chip] = e_send[0]
     rest = pl.ds(1, chips - 1)
     all_back = pltpu.make_async_remote_copy(
-        src_ref=e_send.at[:, rest], dst_ref=e_recv.at[:, rest], send_sem=e_ssem, recv_sem=e_rsem,
+        src_ref=e_send.at[rest], dst_ref=e_recv.at[rest], send_sem=e_ssem, recv_sem=e_rsem,
         device_id=tp_id(1), device_id_type=MESH,
     )
     all_back.wait_recv()
@@ -353,15 +366,23 @@
     out_ref[...] = (resid.astype(F32) + mix).astype(BF16)
 
     pltpu.make_async_remote_copy(
-        src_ref=b_send.at[:, rest], dst_ref=here.at[:, rest], send_sem=b_ssem, recv_sem=b_rsem.at[0],
+        src_ref=b_send.at[rest], dst_ref=here.at[rest], send_sem=b_ssem, recv_sem=b_rsem.at[0],
         device_id=tp_id(1), device_id_type=MESH,
     ).wait_send()
     all_back.wait_send()
-    for d in order:
-        a_copies[d].wait_send()
-    for copies in (g_copies, f_copies, d_copies, x_copies):
-        for copy in copies.values():
-            copy.wait_send()
+    a_all.wait_send()
+    three = pl.ds(0, n_tp - 1)
+    for block, sem in (
+        (rows.at[three, core, groups[0]], g_ssem.at[0]),
+        (rows.at[three, :, groups[1]], g_ssem.at[1]),
+        (rows.at[:, core, groups[0]], f_ssem.at[0]),
+        (here.at[groups[1]], f_ssem.at[1]),
+        (d_send, d_ssem),
+        (x_send.at[three], x_ssem),
+    ):
+        pltpu.make_async_remote_copy(
+            src_ref=block, dst_ref=block, send_sem=sem, recv_sem=sem, device_id=tp_id(1), device_id_type=MESH
+        ).wait_send()
 
 
 def body(
@@ -377,8 +398,10 @@
         expert_gate.swapaxes(1, 2), expert_up.swapaxes(1, 2), expert_down,
     )
     dma = pltpu.SemaphoreType.DMA
-    blocks = (2, chips, 2, width // 2)
-    held = [jax.ShapeDtypeStruct((model, 512), BF16) if a is w_query else a for a in args if a is not w_key and a is not w_value]
+    blocks = (chips, 2, 2, width // 2)
+    held = list(args)
+    held[3:6] = [jax.ShapeDtypeStruct((model, 512), BF16)]
+    held[10:12] = [jax.ShapeDtypeStruct((2,) + args[12].shape[1:], BF16)]
     scratch = [pltpu.VMEM(a.shape, a.dtype) for a in held] + [
         pltpu.VMEM((n_rows, head_gain.shape[0]), F32),
         pltpu.VMEM((n_tp, n_rows, width), BF16),
@@ -392,14 +415,14 @@
         pltpu.VMEM((n_tp, 2 * chips, width), BF16),
         pltpu.VMEM(blocks, BF16),
         pltpu.VMEM(blocks, BF16),
-        dma((len(args) + 2,)),
+        dma((8,)),
         pltpu.SemaphoreType.REGULAR,
-        dma((n_tp,)), dma((n_tp,)),
+        dma, dma,
         dma, dma((2,)),
-        dma((3, n_tp)), dma((3, n_tp)),
-        dma((2, n_tp)), dma((2, n_tp)),
-        dma((n_tp,)), dma((n_tp,)),
-        dma((2, n_tp)), dma((2, n_tp)),
+        dma((2,)), dma((2, n_tp)),
+        dma((2,)), dma((n_tp + 1,)),
+        dma, dma((n_tp,)),
+        dma, dma((3,)),
         dma, dma,
     ]
     return pl.pallas_call(

time: 43.6 us -> 42.7 us (0.979)
  Pallas kernels: 42.9 us -> 41.9 us
    pallas_call x1, Pallas kernels: 42.9 us -> 41.9 us  [body(): pl.pallas_call(functools.partial(kernel, n_ep, n_tp), out_shape=jax.Shape...]
where the time goes in v4:
time: 42.7 us; the launch traced here: 42.5 us
  Pallas kernels  41.9 us (98%)
  local copies, waits for them, and re-layouts  0.6 us (1%)
    pallas_call x1, Pallas kernels, body(): pl.pallas_call(functools.partial(kernel, n_ep, n_tp), out_shape=jax.Shape...  41.9 us

profile of v4, /device:TPU:1, one launch (start us, length us, event | category | flops | bytes accessed | tf_op | source)
XLA Modules:
  0.0 42.5 jit_solution(274246354219877131)
XLA Ops:
  0.0 41.9 %step.1 = bf16[16,256]{1,0:T(8,128)(2,1)S(1)} custom-call(bf16[16,1024]{1,0:T(8,128)(2,1)} %tokens_h.1, s32[1,16]{1,0:T(1,128)} %bitcast.15, f32[1,1024]{1,0:T(1,128)} %bitcast.10, bf16[1024,128]{1,0:T(8,128)(2,1)} %wq_h.1, bf16[1024,128]{1,0:T(8,128)(2,1)} %wk_h.1, bf16[1024,256]{1,0:T(8,128)(2,1)} %wv_h.1, f32[16,1,128,256]{3,2,1,0:T(8,128)} %state_h.1, ...), custom_call_target="tpu_custom_call" | custom-call | tf_op jit(solution)/shard_map/step/pallas_call | solution.py:428
  41.9 0.6 %copy.17 = bf16[16,256]{1,0:T(8,128)(2,1)} copy(bf16[16,256]{1,0:T(8,128)(2,1)S(1)} %step.1) | data formatting | bytes 16384
